TPU v7x, 32 devices: a whole 2x2x4 slice. The times are simulated.
32 devices in a mesh: kv: 8 (over z, y), tp: 4 (over x, core).
Axes of the slice: x: 2, y: 2, z: 4, core: 2. Of those that a mesh axis runs over, the one named last changes fastest.
Arguments:
- inputs: bfloat16 [256, 4096], P(None, 'kv'), may hold values from -150 to 150
- norm_gain: bfloat16 [4096], P('kv'), may hold values from 0.099609375 to 1.8984375
- w_query: bfloat16 [4096, 2048], P('kv', 'tp'), may hold values from -0.09375 to 0.09375
- w_forget: bfloat16 [4096, 2048], P('kv', 'tp'), may hold values from -0.09375 to 0.09375
- w_value: bfloat16 [4096, 2048], P('kv', 'tp'), may hold values from -0.09375 to 0.09375
- lower_bound: float32 [2048], P('tp'), may hold values from 0.05 to 0.9
- head_gain: float32 [2048], P('tp'), may hold values from 0.1 to 1.9
- w_out: bfloat16 [2048, 4096], P('tp', 'kv'), may hold values from -0.125 to 0.125
- prior_state: float32 [64, 16, 128, 128], P('kv', 'tp'), may hold values from -3 to 3
- prev_forget: float32 [64, 4, 2048], P('kv', None, 'tp'), may hold values from 0.3 to 0.97
- prev_values: bfloat16 [64, 4, 2048], P('kv', None, 'tp'), may hold values from -6 to 6
- accepted: int32 [64], P('kv'), may hold values from 0 to 4
Outputs:
- mixed_out: bfloat16 [256, 4096], P(None, ('kv', 'tp'))
- base_state: float32 [64, 16, 128, 128], P('kv', 'tp')
All inputs are finite; a program needn't handle non-finite values.
Results may differ from a plain program's by a relative error of at most 0.01.
Values may be sent and summed in bfloat16 or wider, within the bound.
No kernel may reach another device: no remote copies, remote signals or barrier semaphores. Data moves between devices by JAX's collectives and lax.ppermute only.
A program may use at most 64 MiB of HBM per device.

v0:
```python
import functools

import jax
import jax.numpy as jnp
from jax import lax
from jax.experimental import pallas as pl
from jax.experimental.pallas import tpu as pltpu
from jax.sharding import PartitionSpec as P


EPSILON = 1e-06
LANES = 128
SUBLANES = 8
PACK = 16
PAIR = 2
GROUP = 4


f32 = jnp.float32
bf16 = jnp.bfloat16
VMEM = pltpu.VMEM
WHOLE = pl.BlockSpec(memory_space=pltpu.VMEM)


def grant(mib):
    return pltpu.CompilerParams(vmem_limit_bytes=mib << 20)


def in_hbm(*arrays):
    return [pltpu.with_memory_space_constraint(a, pltpu.HBM) for a in arrays]


def round_up(n, m):
    return -(-n // m) * m


def square_rows(tokens):
    return round_up(tokens, LANES) // LANES


def coded_rows(tokens):
    return round_up(2 * square_rows(tokens), SUBLANES)


def coded(spread):
    rows = spread.shape[0]
    high = spread.astype(bf16).astype(f32)
    parts = [high, spread - high]
    pad = round_up(2 * rows, SUBLANES) - 2 * rows
    if pad:
        parts.append(jnp.zeros((pad, LANES), f32))
    return jnp.concatenate(parts, axis=0).astype(bf16)


def decoded(ref, start, rows):
    tile = ref[start : start + round_up(2 * rows, SUBLANES), :].astype(f32)
    return tile[:rows] + tile[rows : 2 * rows]


def split(x):
    high = x.astype(bf16)
    return high, (x - high.astype(f32)).astype(bf16)


def project_kernel(outer, x_hbm, gain_hbm, wq_hbm, wf_hbm, wv_hbm, *rest):
    across_ref, stay_ref, squares_ref, own_ref = rest[:4]
    ahead = rest[4 : 3 + outer]
    x_ref, gain_ref, w_ref, terms_ref, sems = rest[3 + outer :]
    tokens, features = x_ref.shape
    cols = wq_hbm.shape[1]
    blocks = cols // LANES
    local = tokens // (outer * PAIR)
    copies = [
        pltpu.make_async_copy(x_hbm, x_ref, sems.at[0]),
        pltpu.make_async_copy(gain_hbm, gain_ref, sems.at[1]),
    ]
    for j, w in enumerate((wf_hbm, wv_hbm, wq_hbm)):
        copies.append(pltpu.make_async_copy(w, w_ref.at[j], sems.at[2 + j]))
    for c in copies:
        c.start()
    copies[0].wait()
    copies[1].wait()
    wide = x_ref[...].astype(f32)
    scaled = (wide * gain_ref[...].astype(f32).reshape(1, features)).astype(bf16)
    me = lax.axis_index("kv")
    mine = lax.rem(me, PAIR)
    here = me // PAIR
    nears, fars = [], []
    for k in range(outer):
        there = target(here, k, outer) * PAIR
        nears.append(pl.ds(pl.multiple_of((there + mine) * local, PACK), local))
        fars.append(pl.ds(pl.multiple_of((there + 1 - mine) * local, PACK), local))
    for j in range(3):
        copies[2 + j].wait()
        terms = jnp.dot(scaled, w_ref[j], preferred_element_type=f32)
        for b in range(blocks):
            terms_ref[j * blocks + b] = terms[:, b * LANES : (b + 1) * LANES]
        if j == 2:
            break
        for k in range(outer):
            for b in range(j * blocks, (j + 1) * blocks):
                at = pl.ds((k * 2 * blocks + b) * local, local)
                stay_ref[at, :] = terms_ref[b, nears[k], :]
                across_ref[at, :] = terms_ref[b, fars[k], :].astype(bf16)
        if j == 0:
            squares = wide * wide
            folded = squares[:, :LANES]
            for b in range(1, features // LANES):
                folded = folded + squares[:, b * LANES : (b + 1) * LANES]
            row = jnp.sum(folded.T, axis=0, keepdims=True)
            rows = square_rows(tokens)
            spread = jnp.concatenate(
                [row[:, r * LANES : (r + 1) * LANES] for r in range(rows)], axis=0
            )
            squares_ref[...] = spread
            across_ref[outer * 2 * blocks * local :, :] = coded(spread)
    for k in range(outer):
        for b in range(blocks):
            for r, which in enumerate((nears[k], fars[k])):
                at = pl.ds((r * blocks + b) * local, local)
                piece = terms_ref[2 * blocks + b, which, :]
                if k:
                    ahead[k - 1][at, :] = piece.astype(bf16)
                else:
                    own_ref[at, :] = piece


def project(inputs, norm_gain, w_query, w_forget, w_value, outer):
    tokens, features = inputs.shape
    cols = w_query.shape[1]
    blocks = cols // LANES
    local = tokens // (outer * PAIR)
    section = 2 * blocks * local
    shapes = [
        jax.ShapeDtypeStruct((outer * section + coded_rows(tokens), LANES), bf16),
        jax.ShapeDtypeStruct((outer * section, LANES), f32),
        jax.ShapeDtypeStruct((square_rows(tokens), LANES), f32),
        jax.ShapeDtypeStruct((section, LANES), f32),
    ] + [jax.ShapeDtypeStruct((section, LANES), bf16)] * (outer - 1)
    out = pl.pallas_call(
        functools.partial(project_kernel, outer),
        out_shape=shapes,
        in_specs=[pl.BlockSpec(memory_space=pltpu.HBM)] * 5,
        out_specs=[WHOLE] * len(shapes),
        scratch_shapes=[
            VMEM((tokens, features), bf16),
            VMEM((features,), bf16),
            VMEM((3, features, cols), bf16),
            VMEM((3 * blocks, tokens, LANES), f32),
            pltpu.SemaphoreType.DMA((5,)),
        ],
        compiler_params=grant(24),
        name="project",
    )(*in_hbm(inputs, norm_gain, w_query, w_forget, w_value))
    return out[0], out[1], out[2], out[3], out[4:]


def combine_kernel(outer, after_ref, *refs):
    del after_ref
    across_ref, stay_ref, squares_ref, own_ref = refs[:4]
    ahead = refs[4 : 3 + outer]
    outs = refs[3 + outer :]
    sends, (pair_ref, kept_ref, total_ref, half_ref) = outs[: outer - 1], outs[outer - 1 :]
    rows = squares_ref.shape[0]
    section = kept_ref.shape[0]
    squares = squares_ref[...] + decoded(across_ref, outer * section, rows)
    total_ref[...] = squares
    tail = coded(squares)
    for k in range(1, outer):
        at = pl.ds(k * section, section)
        sends[k - 1][:section, :] = (stay_ref[at, :] + across_ref[at, :].astype(f32)).astype(bf16)
        sends[k - 1][section:, :] = tail
    kept_ref[...] = stay_ref[:section, :] + across_ref[:section, :].astype(f32)
    total = own_ref[...]
    for p in ahead:
        total = total + p[...].astype(f32)
    split_at = half_ref.shape[0]
    half_ref[...] = total[:split_at]
    pair_ref[...] = total[split_at:].astype(bf16)


def combine(after, across, stay, squares, own, ahead, outer):
    section = own.shape[0]
    rows = squares.shape[0]
    height = section + round_up(2 * rows, SUBLANES)
    shapes = [jax.ShapeDtypeStruct((height, LANES), bf16)] * (outer - 1) + [
        jax.ShapeDtypeStruct((section // PAIR, LANES), bf16),
        jax.ShapeDtypeStruct((section, LANES), f32),
        jax.ShapeDtypeStruct((rows, LANES), f32),
        jax.ShapeDtypeStruct((section // PAIR, LANES), f32),
    ]
    out = pl.pallas_call(
        functools.partial(combine_kernel, outer),
        out_shape=shapes,
        in_specs=[WHOLE] * (outer + 4),
        out_specs=[WHOLE] * len(shapes),
        compiler_params=grant(16),
        name="combine",
    )(after, across, stay, squares, own, *ahead)
    return out[: outer - 1], *out[outer - 1 :]


def fold_kernel(
    start, accepted_hbm, after_ref, state_hbm, gate_hbm, value_hbm, base_ref, high_ref, low_ref, *rest
):
    del after_ref
    state_ref, gate_ref, value_ref, left_ref, accepted_ref, sems, gate_sem, value_sem, accepted_sem = rest
    seqs, heads, size, _ = state_ref.shape
    proposals = gate_ref.shape[1]
    gate_copy = pltpu.make_async_copy(gate_hbm.at[pl.ds(start, seqs)], gate_ref, gate_sem)
    value_copy = pltpu.make_async_copy(value_hbm.at[pl.ds(start, seqs)], value_ref, value_sem)
    accepted_copy = pltpu.make_async_copy(accepted_hbm, accepted_ref, accepted_sem)
    accepted_copy.start()
    gate_copy.start()
    value_copy.start()
    loads = [
        pltpu.make_async_copy(state_hbm.at[start + s], state_ref.at[s], sems.at[s])
        for s in range(seqs)
    ]
    for c in loads:
        c.start()
    accepted_copy.wait()
    gate_copy.wait()
    value_copy.wait()
    each = 3 * (proposals + 1)
    depth = round_up(each, PACK)
    none = jnp.zeros((1, size), f32)
    one = jnp.ones((1, size), f32)
    fill = [none] * (depth - each)
    side = jnp.concatenate(([none] * proposals + [one]) * 3 + fill, axis=0)
    for s in range(seqs):
        taken = accepted_ref[start + s]
        gates = gate_ref[s]
        total = jnp.ones_like(gates[:1])
        weights = [None] * proposals
        for j in reversed(range(proposals)):
            use = j < taken
            gate = gates[j : j + 1]
            weights[j] = jnp.where(use, (1.0 - gate) * total, 0.0)
            total = jnp.where(use, gate * total, total)
        exact = jnp.concatenate(weights + [total], axis=0)
        first = exact.astype(bf16).astype(f32)
        second = (exact - first).astype(bf16).astype(f32)
        third = exact - first - second
        pad = [jnp.zeros((depth - each, exact.shape[1]), f32)] if depth > each else []
        left = jnp.concatenate([first, second, third] + pad, axis=0)
        left = jnp.concatenate([left[:, h * size : (h + 1) * size] for h in range(heads)], axis=0)
        left_ref[s] = left.T.astype(bf16)
    rows = lax.broadcasted_iota(jnp.int32, (heads * depth, 2 * size), 0) // depth
    for s in range(seqs):
        if s % GROUP == 0:
            for c in loads[s : s + GROUP]:
                c.wait()
        values = value_ref[s].astype(f32)
        left = left_ref[s]
        for h in range(heads):
            mine = values[:, h * size : (h + 1) * size]
            block = jnp.concatenate([mine, none] * 3 + fill, axis=0)
            block = jnp.concatenate((block, side), axis=1)
            right = jnp.where(rows == h, jnp.concatenate([block] * heads, axis=0), 0.0)
            both = jnp.dot(left, right.astype(bf16), preferred_element_type=f32)
            base = both[:, size:] * state_ref[s, h] + both[:, :size]
            base_ref[s, h] = base
            high, low = split(base)
            high_ref[s, h] = high
            low_ref[s, h] = low


def fold(start, seqs, accepted, after, prior_state, prev_forget, prev_values):
    heads, size = prior_state.shape[1:3]
    proposals, cols = prev_forget.shape[1:]
    shape = (seqs, heads, size, size)
    hbm = pl.BlockSpec(memory_space=pltpu.HBM)
    return pl.pallas_call(
        functools.partial(fold_kernel, start),
        out_shape=[
            jax.ShapeDtypeStruct(shape, f32),
            jax.ShapeDtypeStruct(shape, bf16),
            jax.ShapeDtypeStruct(shape, bf16),
        ],
        in_specs=[hbm, pl.BlockSpec(memory_space=pl.ANY)] + [hbm] * 3,
        out_specs=[WHOLE] * 3,
        scratch_shapes=[
            VMEM(shape, f32),
            VMEM((seqs, proposals, cols), f32),
            VMEM((seqs, proposals, cols), bf16),
            VMEM((seqs, size, heads * round_up(3 * (proposals + 1), PACK)), bf16),
            pltpu.SMEM(accepted.shape, jnp.int32),
            pltpu.SemaphoreType.DMA((seqs,)),
            pltpu.SemaphoreType.DMA,
            pltpu.SemaphoreType.DMA,
            pltpu.SemaphoreType.DMA,
        ],
        cost_estimate=pl.CostEstimate(
            flops=1_000_000_000, bytes_accessed=12 * prior_state.size, transcendentals=0
        ),
        compiler_params=grant(16),
        name="fold",
    )(*in_hbm(accepted), after, *in_hbm(prior_state, prev_forget, prev_values))


def store_kernel(count, after_ref, *refs):
    del after_ref
    bases, out_hbm, sems = refs[:count], refs[count], refs[count + 1]
    copies = []
    for base_ref in bases:
        for s in range(base_ref.shape[0]):
            place = len(copies)
            copies.append(
                pltpu.make_async_copy(base_ref.at[s], out_hbm.at[place], sems.at[place])
            )
    for c in copies:
        c.start()
    for c in copies:
        c.wait()


def store(after, bases):
    seqs = sum(base.shape[0] for base in bases)
    shape = (seqs, *bases[0].shape[1:])
    return pl.pallas_call(
        functools.partial(store_kernel, len(bases)),
        out_shape=jax.ShapeDtypeStruct(shape, f32),
        in_specs=[WHOLE] * (1 + len(bases)),
        out_specs=pl.BlockSpec(memory_space=pltpu.HBM),
        scratch_shapes=[pltpu.SemaphoreType.DMA((seqs,))],
        cost_estimate=pl.CostEstimate(
            flops=1_000_000_000, bytes_accessed=8 * seqs, transcendentals=0
        ),
        compiler_params=grant(8),
        name="store",
    )(after, *bases)


def recur_kernel(seqs, proposals, width, count, *refs):
    kept_ref, squares_ref, half_ref, other_ref = refs[:4]
    highs_ref, lows_ref = refs[4 : 4 + count], refs[4 + count : 4 + 2 * count]
    arrived = refs[4 + 2 * count : -5]
    floor_ref, gain_ref, out_ref, sum_ref, rows_ref = refs[-5:]
    heads, size = highs_ref[0].shape[1:3]
    local = seqs * proposals
    rows = squares_ref.shape[0]
    section = kept_ref.shape[0]
    total = kept_ref[...]
    squares = squares_ref[...]
    for p in arrived:
        total = total + p[:section, :].astype(f32)
        squares = squares + decoded(p, section, rows)
    first = half_ref[...] + other_ref[...].astype(f32)
    me = lax.axis_index("kv")
    lane = lax.broadcasted_iota(jnp.int32, (local, LANES), 1)
    token = lax.broadcasted_iota(jnp.int32, (local, LANES), 0) + me * local
    picked = jnp.zeros((local, LANES), f32)
    for r in range(rows):
        picked = jnp.where(lane + r * LANES == token, squares[r : r + 1], picked)
    column = jnp.sum(picked, axis=1, keepdims=True)
    scale = lax.rsqrt(column / width + EPSILON)
    for b in range(heads):
        sum_ref[b * local : (b + 1) * local, :] = first[b * local : (b + 1) * local] * scale
    for b in range(2 * heads):
        at = slice((heads + b) * local, (heads + b + 1) * local)
        sum_ref[at, :] = total[b * local : (b + 1) * local] * scale
    for h in range(heads):
        at = slice(h * size, (h + 1) * size)

        def take(kind, t):
            return sum_ref[pl.ds((kind * heads + h) * local + t, seqs, stride=proposals), :]

        floor = floor_ref[:, at]
        head_gain = gain_ref[:, at]
        query, forget, key, value = [], [], [], []
        for t in range(proposals):
            q = take(0, t)
            query.append(q / (1.0 + jnp.exp(-q)))
            g = floor + (1.0 - floor) / (1.0 + jnp.exp(-take(1, t)))
            forget.append(g)
            key.append(1.0 - g)
            value.append(take(2, t))
        lefts = []
        mixes = []
        for t in range(proposals):
            carried = query[t]
            mix = None
            for j in reversed(range(t + 1)):
                weight = jnp.sum(carried * key[j], axis=1, keepdims=True) * value[j]
                mix = weight if mix is None else mix + weight
                carried = carried * forget[j]
            lefts.append(carried)
            mixes.append(mix)
        highs = [x.astype(bf16).astype(f32) for x in lefts]
        lows = [x - y for x, y in zip(lefts, highs)]
        both = jnp.concatenate(highs + lows, axis=0)
        sub_all = lax.broadcasted_iota(jnp.int32, both.shape, 0) % seqs
        left = jnp.concatenate(
            [jnp.where(sub_all == s, both, 0.0).astype(bf16) for s in range(seqs)], axis=1
        )
        high = jnp.concatenate([r[:, h].reshape(-1, size) for r in highs_ref], axis=0)
        low = jnp.concatenate([r[:, h].reshape(-1, size) for r in lows_ref], axis=0)
        first = jnp.dot(left, high, preferred_element_type=f32)
        second = jnp.dot(left[:local], low, preferred_element_type=f32)
        read = first[:local] + first[local:] + second
        for t in range(proposals):
            result = read[t * seqs : (t + 1) * seqs] + mixes[t]
            mean = jnp.sum(result * result, axis=1, keepdims=True) / size
            rows_ref[pl.ds(h * local + t, seqs, stride=proposals), :] = (
                result * lax.rsqrt(mean + EPSILON) * head_gain
            )
        out_ref[:, at] = rows_ref[h * local : (h + 1) * local, :].astype(bf16)


def recur(kept, squares, half, other, highs, lows, arrived, lower_bound, head_gain, proposals, width):
    count = len(highs)
    seqs = sum(h.shape[0] for h in highs)
    heads, size = highs[0].shape[1:3]
    local = seqs * proposals
    cols = heads * size
    return pl.pallas_call(
        functools.partial(recur_kernel, seqs, proposals, width, count),
        out_shape=jax.ShapeDtypeStruct((local, cols), bf16),
        in_specs=[WHOLE] * (len(arrived) + 6 + 2 * count),
        out_specs=WHOLE,
        scratch_shapes=[VMEM((3 * heads * local, size), f32), VMEM((heads * local, size), f32)],
        compiler_params=grant(16),
        name="recur",
    )(
        kept,
        squares,
        half,
        other,
        *highs,
        *lows,
        *arrived,
        lower_bound.reshape(1, cols),
        head_gain.reshape(1, cols),
    )


def stack_kernel(count, *refs):
    pieces, out_ref = refs[:count], refs[count]
    local = pieces[0].shape[0]
    for k in range(count):
        out_ref[k * local : (k + 1) * local, :] = pieces[k][...]


def stack(pieces):
    count = len(pieces)
    local, cols = pieces[0].shape
    return pl.pallas_call(
        functools.partial(stack_kernel, count),
        out_shape=jax.ShapeDtypeStruct((count * local, cols), bf16),
        in_specs=[WHOLE] * count,
        out_specs=WHOLE,
        compiler_params=grant(8),
        name="stack",
    )(*pieces)


def mix_kernel(groups, own_ref, others_ref, near_w_ref, upper_ref, lower_ref, keep_ref, send_ref, cols_ref):
    half = groups // PAIR
    height = own_ref.shape[0] + others_ref.shape[0]
    left = jnp.concatenate((own_ref[...], others_ref[...]), axis=0)
    span = near_w_ref.shape[1] // groups
    far_w = jnp.concatenate((upper_ref[...], lower_ref[...]), axis=0)
    for side, w in enumerate((near_w_ref[...], far_w)):
        partial = jnp.dot(left, w, preferred_element_type=f32)
        for g in range(groups):
            cols_ref[side, g] = partial[:, g * span : (g + 1) * span]
    me = lax.axis_index("tp")
    mine = lax.rem(me, PAIR)
    for side in range(PAIR):
        for k in range(half):
            group = target(me // PAIR, k, half) * PAIR
            at = pl.ds((side * half + k) * height, height)
            keep_ref[at, :] = cols_ref[side, group + mine]
            send_ref[at, :] = cols_ref[side, group + 1 - mine].astype(bf16)


def mix(own, others, near_w, upper, lower, groups):
    height = own.shape[0] + others.shape[0]
    span = near_w.shape[1] // groups
    return pl.pallas_call(
        functools.partial(mix_kernel, groups),
        out_shape=[
            jax.ShapeDtypeStruct((groups * height, span), f32),
            jax.ShapeDtypeStruct((groups * height, span), bf16),
        ],
        in_specs=[WHOLE] * 5,
        out_specs=[WHOLE] * 2,
        scratch_shapes=[VMEM((PAIR, groups, height, span), f32)],
        compiler_params=grant(16),
        name="mix",
    )(own, others, near_w, upper, lower)


def join_kernel(keep_ref, other_ref, own_ref, *outs):
    height = own_ref.shape[0]
    total = keep_ref[...] + other_ref[...].astype(f32)
    own_ref[...] = total[:height]
    for i, out in enumerate(outs):
        out[...] = total[(i + 1) * height : (i + 2) * height].astype(bf16)


def join(keep, other, groups):
    height, span = keep.shape[0] // groups, keep.shape[1]
    out = pl.pallas_call(
        join_kernel,
        out_shape=[jax.ShapeDtypeStruct((height, span), f32)]
        + [jax.ShapeDtypeStruct((height, span), bf16)] * (groups - 1),
        in_specs=[WHOLE] * 2,
        out_specs=[WHOLE] * groups,
        compiler_params=grant(8),
        name="join",
    )(keep, other)
    return out[0], out[1:]


def finish_kernel(outer, groups, *refs):
    out_ref = refs[-1]
    half = groups // PAIR
    local = refs[0].shape[0] // outer
    me = lax.axis_index("kv")
    here = me // PAIR
    mine = lax.rem(me, PAIR)
    for side, pieces in ((mine, refs[:half]), (1 - mine, refs[half:groups])):
        total = pieces[0][...].astype(f32)
        for p in pieces[1:]:
            total = total + p[...].astype(f32)
        total = total.astype(bf16)
        for i, k in enumerate([0] + far_first(outer)):
            place = (origin(here, k, outer) * PAIR + side) * local
            out_ref[pl.ds(pl.multiple_of(place, PACK), local), :] = total[i * local : (i + 1) * local]


def finish(pieces, outer):
    groups = len(pieces)
    height, span = pieces[0].shape
    return pl.pallas_call(
        functools.partial(finish_kernel, outer, groups),
        out_shape=jax.ShapeDtypeStruct((PAIR * height, span), bf16),
        in_specs=[WHOLE] * groups,
        out_specs=WHOLE,
        compiler_params=grant(8),
        name="finish",
    )(*pieces)


def target(here, k, count):
    return here ^ k if count & (count - 1) == 0 else (here + k) % count


def origin(here, k, count):
    return here ^ k if count & (count - 1) == 0 else (here + count - k) % count


def far_first(count):
    return sorted(range(1, count), key=lambda k: -k)


def across_groups(x, k, groups, parts, other):
    half = groups // PAIR
    moves = []
    for s in range(parts):
        to = s - s % PAIR + (s + other) % PAIR
        for g in range(groups):
            there = target(g // PAIR, k, half) * PAIR + g % PAIR
            moves.append((s * groups + g, to * groups + there))
    return lax.ppermute(x, ("kv", "tp"), moves)


def swap(x, axis, count):
    return lax.ppermute(x, axis, [(s, s - s % PAIR + (s + 1) % PAIR) for s in range(count)])


def along(x, k, parts):
    count = parts // PAIR
    return lax.ppermute(
        x, "kv", [(s, PAIR * target(s // PAIR, k, count) + s % PAIR) for s in range(parts)]
    )


def body(
    parts,
    groups,
    inputs,
    norm_gain,
    w_query,
    w_forget,
    w_value,
    lower_bound,
    head_gain,
    w_out,
    prior_state,
    prev_forget,
    prev_values,
    accepted,
):
    width = inputs.shape[1] * parts
    outer = parts // PAIR
    order = far_first(outer)
    across, stay, squares, own, ahead = project(
        inputs, norm_gain, w_query, w_forget, w_value, outer
    )
    across = swap(across, "kv", parts)
    moved = []
    for k in order:
        moved.append(along(ahead[k - 1], k, parts))
    ahead = moved
    cut = w_out.shape[0] // 2
    upper = swap(w_out[:cut], "kv", parts)
    state = (prior_state, prev_forget, prev_values)
    seqs = prior_state.shape[0]
    early = seqs // 2
    base, high, low = fold(0, early, accepted, stay, *state)
    sends, pair, kept, squares, half = combine(
        low, across, stay, squares, own, ahead, outer
    )
    late_base, late_high, late_low = fold(early, seqs - early, accepted, pair, *state)
    arrived = []
    for k in order:
        arrived.append(along(sends[k - 1], k, parts))
    base_state = store(pair, (base, late_base))
    other = swap(pair, "kv", parts)
    lower = swap(w_out[cut:], "kv", parts)
    normed = recur(
        kept,
        squares,
        half,
        other,
        (high, late_high),
        (low, late_low),
        arrived,
        lower_bound,
        head_gain,
        prev_forget.shape[1],
        width,
    )
    column = []
    for k in order:
        column.append(along(normed, k, parts))
    near = stack(column)
    keep, send = mix(normed, near, w_out, upper, lower, groups)
    own, sends = join(keep, swap(send, "tp", groups), groups)
    half = groups // PAIR
    pieces = [own] + [None] * (groups - 1)
    for i in reversed(range(1, groups)):
        pieces[i] = across_groups(sends[i - 1], i % half, groups, parts, i // half)
    return finish(pieces, outer), base_state


def solution(mesh):
    in_specs = (
        P(None, "kv"),
        P("kv"),
        P("kv", "tp"),
        P("kv", "tp"),
        P("kv", "tp"),
        P("tp"),
        P("tp"),
        P("tp", "kv"),
        P("kv", "tp", None, None),
        P("kv", None, "tp"),
        P("kv", None, "tp"),
        P("kv"),
    )
    out_specs = (P(None, ("kv", "tp")), P("kv", "tp", None, None))
    step = functools.partial(body, mesh.shape["kv"], mesh.shape["tp"])
    step = jax.shard_map(step, mesh=mesh, in_specs=in_specs, out_specs=out_specs, check_vma=False)
    return step
```

profile of v0, /device:TPU:0, one launch (start us, length us, event | category | flops | bytes accessed | tf_op | source)
XLA Modules:
  0.0 48.3 jit_solution(9763572332297513412)
XLA Ops:
  0.6 0.0 copy-start
  0.6 2.2 %project.1 = (bf16[1032,128]{1,0:T(8,128)(2,1)S(1)}, f32[1024,128]{1,0:T(8,128)S(1)}, f32[2,128]{1,0:T(2,128)S(1)}, f32[256,128]{1,0:T(8,128)S(1)}, bf16[256,128...) custom-call(bf16[256,512]{1,0:T(8,128)(2,1)} %x_hbm.1, bf16[512]{0:T(512)(128)(2,1)} %gain_hbm.1, ...), custom_call_target="tpu_custom_call" | custom-call | tf_op jit(solution)/shard_map/project/pallas_call | solution.py:140
  2.9 3.1 %collective-permute-start = (bf16[1032,128]{1,0:T(8,128)(2,1)S(1)}, bf16[1032,128]{1,0:T(8,128)(2,1)S(1)}, u32[]{:S(2)}, u32[]{:S(2)}) collective-permute-start(bf16[1032,128]{1,0:T(8,128)(2,1)S(1)} %get-tuple-element.30), channel_id=1, source_target_pairs={{0,4},{4,0},{8,12},{12,8},{16,20},{20,16},{24,28},{28,24},{1,5},{5... | collective-permute-start | bytes 792584 | tf_op jit(solution)/shard_map/ppermute | solution.py:571
  6.0 3.6 %collective-permute-start.1 = (bf16[256,128]{1,0:T(8,128)(2,1)S(1)}, bf16[256,128]{1,0:T(8,128)(2,1)S(1)}, u32[]{:S(2)}, u32[]{:S(2)}) collective-permute-start(bf16[256,128]{1,0:T(8,128)(2,1)S(1)} %get-tuple-element.33), channel_id=1, source_target_pairs={{0,24},{4,28},{8,16},{12,20},{16,8},{20,12},{24,0},{28,4},{1,25},{... | collective-permute-start | bytes 196616 | tf_op jit(solution)/shard_map/ppermute | solution.py:576
  9.6 0.0 copy-done
  9.6 0.6 %collective-permute-start.11 = (bf16[256,512]{1,0:T(8,128)(2,1)S(1)}, bf16[256,512]{1,0:T(8,128)(2,1)S(1)}, u32[]{:S(2)}, u32[]{:S(2)}) collective-permute-start(bf16[256,512]{1,0:T(8,128)(2,1)S(1)} %get-tuple-element.55), channel_id=1, source_target_pairs={{0,4},{4,0},{8,12},{12,8},{16,20},{20,16},{24,28},{28,24},{1,5},{5... | collective-permute-start | bytes 786440 | tf_op jit(solution)/shard_map/ppermute | solution.py:571
  10.2 1.5 %collective-permute-start.12 = (bf16[256,512]{1,0:T(8,128)(2,1)S(1)}, bf16[256,512]{1,0:T(8,128)(2,1)S(1)}, u32[]{:S(2)}, u32[]{:S(2)}) collective-permute-start(bf16[256,512]{1,0:T(8,128)(2,1)S(1)} %get-tuple-element.54), channel_id=1, source_target_pairs={{0,4},{4,0},{8,12},{12,8},{16,20},{20,16},{24,28},{28,24},{1,5},{5... | collective-permute-start | bytes 786440 | tf_op jit(solution)/shard_map/ppermute | solution.py:571
  11.7 0.0 collective-permute-start.2
  11.7 0.4 collective-permute-done.1.refs_4_
  12.1 0.4 collective-permute-start.3
  12.5 1.7 %fold.2 = (f32[4,4,128,128]{3,2,1,0:T(8,128)S(1)}, bf16[4,4,128,128]{3,2,1,0:T(8,128)(2,1)S(1)}, bf16[4,4,128,128]{3,2,1,0:T(8,128)(2,1)S(1)}) custom-call(s32[8]{0:T(128)} %accepted_hbm.3, f32[1024,128]{1,0:T(8,128)S(1)} %get-tuple-element.28.after_ref.refs_1_, f32[8,4,128,128]{3,2,1,0:T(8,128)} %state_hbm.3, f32[8,4,512]{2,1,0:T(4,128)} %gate_hbm.3, ...), custom_call_target="tpu_custom_call" | custom-call | flops 1000000000 | bytes 6291456 | tf_op jit(solution)/shard_map/fold/pallas_call | solution.py:274
  14.2 2.8 %collective-permute-done.2.refs_5_ = bf16[256,128]{1,0:T(8,128)(2,1)S(1)} collective-permute-done((bf16[256,128]{1,0:T(8,128)(2,1)S(1)}, bf16[256,128]{1,0:T(8,128)(2,1)S(1)}, u32[]{:S(2)}, u32[]{:S(2)}) %collective-permute-start.2) | collective-permute-done | bytes 65568 | tf_op jit(solution)/shard_map/ppermute | solution.py:576
  17.1 0.0 collective-permute-done.3.refs_6_
  17.1 0.0 collective-permute-done.refs_0_
  17.1 0.1 combine.1
  17.1 0.0 copy-start.1
  17.2 0.0 copy-start.2
  17.2 0.6 %collective-permute-start.4 = (bf16[128,128]{1,0:T(8,128)(2,1)S(1)}, bf16[128,128]{1,0:T(8,128)(2,1)S(1)}, u32[]{:S(2)}, u32[]{:S(2)}) collective-permute-start(bf16[128,128]{1,0:T(8,128)(2,1)S(1)} %get-tuple-element.39.after_ref), channel_id=1, source_target_pairs={{0,4},{4,0},{8,12},{12,8},{16,20},{20,16},{24,28},{28,24},{1,5},{5... | collective-permute-start | bytes 98312 | tf_op jit(solution)/shard_map/ppermute | solution.py:571
  17.7 3.5 %collective-permute-start.5 = (bf16[264,128]{1,0:T(8,128)(2,1)S(1)}, bf16[264,128]{1,0:T(8,128)(2,1)S(1)}, u32[]{:S(2)}, u32[]{:S(2)}) collective-permute-start(bf16[264,128]{1,0:T(8,128)(2,1)S(1)} %get-tuple-element.43), channel_id=1, source_target_pairs={{0,24},{4,28},{8,16},{12,20},{16,8},{20,12},{24,0},{28,4},{1,25},{... | collective-permute-start | bytes 202760 | tf_op jit(solution)/shard_map/ppermute | solution.py:576
  21.2 0.0 collective-permute-start.6
  21.2 3.0 %collective-permute-done.4.refs_3_ = bf16[128,128]{1,0:T(8,128)(2,1)S(1)} collective-permute-done((bf16[128,128]{1,0:T(8,128)(2,1)S(1)}, bf16[128,128]{1,0:T(8,128)(2,1)S(1)}, u32[]{:S(2)}, u32[]{:S(2)}) %collective-permute-start.4) | collective-permute-done | bytes 32800 | tf_op jit(solution)/shard_map/ppermute | solution.py:571
  24.2 1.8 %collective-permute-start.7 = (bf16[264,128]{1,0:T(8,128)(2,1)S(1)}, bf16[264,128]{1,0:T(8,128)(2,1)S(1)}, u32[]{:S(2)}, u32[]{:S(2)}) collective-permute-start(bf16[264,128]{1,0:T(8,128)(2,1)S(1)} %get-tuple-element.45), channel_id=1, source_target_pairs={{0,8},{4,12},{8,0},{12,4},{16,24},{20,28},{24,16},{28,20},{1,9},{5... | collective-permute-start | bytes 202760 | tf_op jit(solution)/shard_map/ppermute | solution.py:576
  26.0 1.7 %fold.3 = (f32[4,4,128,128]{3,2,1,0:T(8,128)S(1)}, bf16[4,4,128,128]{3,2,1,0:T(8,128)(2,1)S(1)}, bf16[4,4,128,128]{3,2,1,0:T(8,128)(2,1)S(1)}) custom-call(s32[8]{0:T(128)} %accepted_hbm.3, bf16[128,128]{1,0:T(8,128)(2,1)S(1)} %get-tuple-element.39.after_ref, f32[8,4,128,128]{3,2,1,0:T(8,128)} %state_hbm.3, f32[8,4,512]{2,1,0:T(4,128)} %gate_hbm.3, ...), custom_call_target="tpu_custom_call" | custom-call | flops 1000000000 | bytes 6291456 | tf_op jit(solution)/shard_map/fold/pallas_call | solution.py:274
  27.7 0.0 collective-permute-done.5.refs_8_
  27.7 0.0 collective-permute-done.6.refs_9_
  27.8 0.8 %collective-permute-done.7.refs_10_ = bf16[264,128]{1,0:T(8,128)(2,1)S(1)} collective-permute-done((bf16[264,128]{1,0:T(8,128)(2,1)S(1)}, bf16[264,128]{1,0:T(8,128)(2,1)S(1)}, u32[]{:S(2)}, u32[]{:S(2)}) %collective-permute-start.7) | collective-permute-done | bytes 67616 | tf_op jit(solution)/shard_map/ppermute | solution.py:576
  28.5 0.0 copy-done.1
  28.5 0.0 copy-done.2
  28.5 0.7 %recur.1.own_ref = bf16[32,512]{1,0:T(8,128)(2,1)S(1)} custom-call(f32[256,128]{1,0:T(8,128)S(1)} %get-tuple-element.36.refs_0_, f32[2,128]{1,0:T(2,128)S(1)} %get-tuple-element.37.refs_1_, f32[128,128]{1,0:T(8,128)S(1)} %get-tuple-element.38.refs_2_, bf16[128,128]{1,0:T(8,128)(2,1)S(1)} %collective-permute-done.4.refs_3_, ...), custom_call_target="tpu_custom_call" | custom-call | tf_op jit(solution)/shard_map/recur/pallas_call | solution.py:417
  29.2 3.9 %collective-permute-start.8 = (bf16[32,512]{1,0:T(8,128)(2,1)S(1)}, bf16[32,512]{1,0:T(8,128)(2,1)S(1)}, u32[]{:S(2)}, u32[]{:S(2)}) collective-permute-start(bf16[32,512]{1,0:T(8,128)(2,1)S(1)} %recur.1.own_ref), channel_id=1, source_target_pairs={{0,24},{4,28},{8,16},{12,20},{16,8},{20,12},{24,0},{28,4},{1,25},{... | collective-permute-start | bytes 98312 | tf_op jit(solution)/shard_map/ppermute | solution.py:576
  33.1 0.0 collective-permute-start.9
  33.1 0.6 %collective-permute-start.10 = (bf16[32,512]{1,0:T(8,128)(2,1)S(1)}, bf16[32,512]{1,0:T(8,128)(2,1)S(1)}, u32[]{:S(2)}, u32[]{:S(2)}) collective-permute-start(bf16[32,512]{1,0:T(8,128)(2,1)S(1)} %recur.1.own_ref), channel_id=1, source_target_pairs={{0,8},{4,12},{8,0},{12,4},{16,24},{20,28},{24,16},{28,20},{1,9},{5... | collective-permute-start | bytes 98312 | tf_op jit(solution)/shard_map/ppermute | solution.py:576
  33.7 1.4 %collective-permute-done.8.refs_0_ = bf16[32,512]{1,0:T(8,128)(2,1)S(1)} collective-permute-done((bf16[32,512]{1,0:T(8,128)(2,1)S(1)}, bf16[32,512]{1,0:T(8,128)(2,1)S(1)}, u32[]{:S(2)}, u32[]{:S(2)}) %collective-permute-start.8) | collective-permute-done | bytes 32800 | tf_op jit(solution)/shard_map/ppermute | solution.py:576
  35.1 2.8 %collective-permute-done.9.refs_1_ = bf16[32,512]{1,0:T(8,128)(2,1)S(1)} collective-permute-done((bf16[32,512]{1,0:T(8,128)(2,1)S(1)}, bf16[32,512]{1,0:T(8,128)(2,1)S(1)}, u32[]{:S(2)}, u32[]{:S(2)}) %collective-permute-start.9) | collective-permute-done | bytes 32800 | tf_op jit(solution)/shard_map/ppermute | solution.py:576
  37.9 0.0 collective-permute-done.10.refs_2_
  37.9 0.0 collective-permute-done.11.upper_ref
  37.9 0.0 collective-permute-done.12.lower_ref
  37.9 0.3 mix.1
  38.3 0.1 collective-permute-start.13
  38.4 1.3 %collective-permute-done.13.other_ref = bf16[512,128]{1,0:T(8,128)(2,1)S(1)} collective-permute-done((bf16[512,128]{1,0:T(8,128)(2,1)S(1)}, bf16[512,128]{1,0:T(8,128)(2,1)S(1)}, u32[]{:S(2)}, u32[]{:S(2)}) %collective-permute-start.13) | collective-permute-done | bytes 131104 | tf_op jit(solution)/shard_map/ppermute | solution.py:571
  39.7 1.6 %collective-permute-start.14 = (bf16[128,128]{1,0:T(8,128)(2,1)S(1)}, bf16[128,128]{1,0:T(8,128)(2,1)S(1)}, u32[]{:S(2)}, u32[]{:S(2)}) collective-permute-start(bf16[128,128]{1,0:T(8,128)(2,1)S(1)} %get-tuple-element.49), channel_id=1, source_target_pairs={{0,2},{1,3},{2,0},{3,1},{4,6},{5,7},{6,4},{7,5},{8,10},{9,11},{10,... | collective-permute-start | bytes 98312 | tf_op jit(solution)/shard_map/ppermute | solution.py:567
  41.3 1.5 %collective-permute-start.15 = (bf16[128,128]{1,0:T(8,128)(2,1)S(1)}, bf16[128,128]{1,0:T(8,128)(2,1)S(1)}, u32[]{:S(2)}, u32[]{:S(2)}) collective-permute-start(bf16[128,128]{1,0:T(8,128)(2,1)S(1)} %get-tuple-element.50), channel_id=1, source_target_pairs={{0,4},{1,5},{2,6},{3,7},{4,0},{5,1},{6,2},{7,3},{8,12},{9,13},{10,... | collective-permute-start | bytes 98312 | tf_op jit(solution)/shard_map/ppermute | solution.py:567
  42.8 0.5 collective-permute-start.16
  43.3 1.4 %store.1 = f32[8,4,128,128]{3,2,1,0:T(8,128)} custom-call(bf16[128,128]{1,0:T(8,128)(2,1)S(1)} %get-tuple-element.39.after_ref, f32[4,4,128,128]{3,2,1,0:T(8,128)S(1)} %get-tuple-element.52.refs_0_, f32[4,4,128,128]{3,2,1,0:T(8,128)S(1)} %get-tuple-element.53.refs_1_), custom_call_target="tpu_custom_call" | custom-call | flops 1000000000 | bytes 64 | tf_op jit(solution)/shard_map/store/pallas_call | solution.py:321
  44.7 0.0 collective-permute-done.14.refs_1_
  44.7 0.5 %collective-permute-done.15.refs_2_ = bf16[128,128]{1,0:T(8,128)(2,1)S(1)} collective-permute-done((bf16[128,128]{1,0:T(8,128)(2,1)S(1)}, bf16[128,128]{1,0:T(8,128)(2,1)S(1)}, u32[]{:S(2)}, u32[]{:S(2)}) %collective-permute-start.15) | collective-permute-done | bytes 32800 | tf_op jit(solution)/shard_map/ppermute | solution.py:567
  45.2 2.4 %collective-permute-done.16.refs_3_ = bf16[128,128]{1,0:T(8,128)(2,1)S(1)} collective-permute-done((bf16[128,128]{1,0:T(8,128)(2,1)S(1)}, bf16[128,128]{1,0:T(8,128)(2,1)S(1)}, u32[]{:S(2)}, u32[]{:S(2)}) %collective-permute-start.16) | collective-permute-done | bytes 32800 | tf_op jit(solution)/shard_map/ppermute | solution.py:567
  47.6 0.6 %finish.1 = bf16[256,128]{1,0:T(8,128)(2,1)} custom-call(f32[128,128]{1,0:T(8,128)S(1)} %get-tuple-element.48.refs_0_, bf16[128,128]{1,0:T(8,128)(2,1)S(1)} %collective-permute-done.14.refs_1_, bf16[128,128]{1,0:T(8,128)(2,1)S(1)} %collective-permute-done.15.refs_2_, bf16[128,128]{1,0:T(8,128)(2,1)S(1)} %collective-permute-done.16.refs_3_), custom_call_target="tpu_custom_call" | custom-call | tf_op jit(solution)/shard_map/finish/pallas_call | solution.py:537
  (3 shorter events, 0.1 us)
Async XLA Ops:
  0.6 8.9 %copy-start = (bf16[512,512]{1,0:T(8,128)(2,1)S(1)}, bf16[512,512]{1,0:T(8,128)(2,1)}, u32[]{:S(2)}) copy-start(bf16[512,512]{1,0:T(8,128)(2,1)} %near_w_ref.1) | copy-start | bytes 1572868
  2.9 14.2 %collective-permute-start = (bf16[1032,128]{1,0:T(8,128)(2,1)S(1)}, bf16[1032,128]{1,0:T(8,128)(2,1)S(1)}, u32[]{:S(2)}, u32[]{:S(2)}) collective-permute-start(bf16[1032,128]{1,0:T(8,128)(2,1)S(1)} %get-tuple-element.30), channel_id=1, source_target_pairs={{0,4},{4,0},{8,12},{12,8},{16,20},{20,16},{24,28},{28,24},{1,5},{5... | collective-permute-start | bytes 792584 | tf_op jit(solution)/shard_map/ppermute | solution.py:571
  6.0 6.1 %collective-permute-start.1 = (bf16[256,128]{1,0:T(8,128)(2,1)S(1)}, bf16[256,128]{1,0:T(8,128)(2,1)S(1)}, u32[]{:S(2)}, u32[]{:S(2)}) collective-permute-start(bf16[256,128]{1,0:T(8,128)(2,1)S(1)} %get-tuple-element.33), channel_id=1, source_target_pairs={{0,24},{4,28},{8,16},{12,20},{16,8},{20,12},{24,0},{28,4},{1,25},{... | collective-permute-start | bytes 196616 | tf_op jit(solution)/shard_map/ppermute | solution.py:576
  9.6 28.3 %collective-permute-start.11 = (bf16[256,512]{1,0:T(8,128)(2,1)S(1)}, bf16[256,512]{1,0:T(8,128)(2,1)S(1)}, u32[]{:S(2)}, u32[]{:S(2)}) collective-permute-start(bf16[256,512]{1,0:T(8,128)(2,1)S(1)} %get-tuple-element.55), channel_id=1, source_target_pairs={{0,4},{4,0},{8,12},{12,8},{16,20},{20,16},{24,28},{28,24},{1,5},{5... | collective-permute-start | bytes 786440 | tf_op jit(solution)/shard_map/ppermute | solution.py:571
  10.2 27.8 %collective-permute-start.12 = (bf16[256,512]{1,0:T(8,128)(2,1)S(1)}, bf16[256,512]{1,0:T(8,128)(2,1)S(1)}, u32[]{:S(2)}, u32[]{:S(2)}) collective-permute-start(bf16[256,512]{1,0:T(8,128)(2,1)S(1)} %get-tuple-element.54), channel_id=1, source_target_pairs={{0,4},{4,0},{8,12},{12,8},{16,20},{20,16},{24,28},{28,24},{1,5},{5... | collective-permute-start | bytes 786440 | tf_op jit(solution)/shard_map/ppermute | solution.py:571
  11.7 5.4 %collective-permute-start.2 = (bf16[256,128]{1,0:T(8,128)(2,1)S(1)}, bf16[256,128]{1,0:T(8,128)(2,1)S(1)}, u32[]{:S(2)}, u32[]{:S(2)}) collective-permute-start(bf16[256,128]{1,0:T(8,128)(2,1)S(1)} %get-tuple-element.34), channel_id=1, source_target_pairs={{0,16},{4,20},{8,24},{12,28},{16,0},{20,4},{24,8},{28,12},{1,17},{... | collective-permute-start | bytes 196616 | tf_op jit(solution)/shard_map/ppermute | solution.py:576
  12.1 5.0 %collective-permute-start.3 = (bf16[256,128]{1,0:T(8,128)(2,1)S(1)}, bf16[256,128]{1,0:T(8,128)(2,1)S(1)}, u32[]{:S(2)}, u32[]{:S(2)}) collective-permute-start(bf16[256,128]{1,0:T(8,128)(2,1)S(1)} %get-tuple-element.35), channel_id=1, source_target_pairs={{0,8},{4,12},{8,0},{12,4},{16,24},{20,28},{24,16},{28,20},{1,9},{5... | collective-permute-start | bytes 196616 | tf_op jit(solution)/shard_map/ppermute | solution.py:576
  17.1 11.4 %copy-start.1 = (f32[512]{0:T(512)S(1)}, f32[512]{0:T(512)}, u32[]{:S(2)}) copy-start(f32[512]{0:T(512)} %param.17) | copy-start | bytes 6148
  17.2 11.4 %copy-start.2 = (f32[512]{0:T(512)S(1)}, f32[512]{0:T(512)}, u32[]{:S(2)}) copy-start(f32[512]{0:T(512)} %param.18) | copy-start | bytes 6148
  17.2 7.1 %collective-permute-start.4 = (bf16[128,128]{1,0:T(8,128)(2,1)S(1)}, bf16[128,128]{1,0:T(8,128)(2,1)S(1)}, u32[]{:S(2)}, u32[]{:S(2)}) collective-permute-start(bf16[128,128]{1,0:T(8,128)(2,1)S(1)} %get-tuple-element.39.after_ref), channel_id=1, source_target_pairs={{0,4},{4,0},{8,12},{12,8},{16,20},{20,16},{24,28},{28,24},{1,5},{5... | collective-permute-start | bytes 98312 | tf_op jit(solution)/shard_map/ppermute | solution.py:571
  17.7 10.0 %collective-permute-start.5 = (bf16[264,128]{1,0:T(8,128)(2,1)S(1)}, bf16[264,128]{1,0:T(8,128)(2,1)S(1)}, u32[]{:S(2)}, u32[]{:S(2)}) collective-permute-start(bf16[264,128]{1,0:T(8,128)(2,1)S(1)} %get-tuple-element.43), channel_id=1, source_target_pairs={{0,24},{4,28},{8,16},{12,20},{16,8},{20,12},{24,0},{28,4},{1,25},{... | collective-permute-start | bytes 202760 | tf_op jit(solution)/shard_map/ppermute | solution.py:576
  21.2 6.5 %collective-permute-start.6 = (bf16[264,128]{1,0:T(8,128)(2,1)S(1)}, bf16[264,128]{1,0:T(8,128)(2,1)S(1)}, u32[]{:S(2)}, u32[]{:S(2)}) collective-permute-start(bf16[264,128]{1,0:T(8,128)(2,1)S(1)} %get-tuple-element.44), channel_id=1, source_target_pairs={{0,16},{4,20},{8,24},{12,28},{16,0},{20,4},{24,8},{28,12},{1,17},{... | collective-permute-start | bytes 202760 | tf_op jit(solution)/shard_map/ppermute | solution.py:576
  24.2 4.3 %collective-permute-start.7 = (bf16[264,128]{1,0:T(8,128)(2,1)S(1)}, bf16[264,128]{1,0:T(8,128)(2,1)S(1)}, u32[]{:S(2)}, u32[]{:S(2)}) collective-permute-start(bf16[264,128]{1,0:T(8,128)(2,1)S(1)} %get-tuple-element.45), channel_id=1, source_target_pairs={{0,8},{4,12},{8,0},{12,4},{16,24},{20,28},{24,16},{28,20},{1,9},{5... | collective-permute-start | bytes 202760 | tf_op jit(solution)/shard_map/ppermute | solution.py:576
  29.2 5.9 %collective-permute-start.8 = (bf16[32,512]{1,0:T(8,128)(2,1)S(1)}, bf16[32,512]{1,0:T(8,128)(2,1)S(1)}, u32[]{:S(2)}, u32[]{:S(2)}) collective-permute-start(bf16[32,512]{1,0:T(8,128)(2,1)S(1)} %recur.1.own_ref), channel_id=1, source_target_pairs={{0,24},{4,28},{8,16},{12,20},{16,8},{20,12},{24,0},{28,4},{1,25},{... | collective-permute-start | bytes 98312 | tf_op jit(solution)/shard_map/ppermute | solution.py:576
  33.1 4.8 %collective-permute-start.9 = (bf16[32,512]{1,0:T(8,128)(2,1)S(1)}, bf16[32,512]{1,0:T(8,128)(2,1)S(1)}, u32[]{:S(2)}, u32[]{:S(2)}) collective-permute-start(bf16[32,512]{1,0:T(8,128)(2,1)S(1)} %recur.1.own_ref), channel_id=1, source_target_pairs={{0,16},{4,20},{8,24},{12,28},{16,0},{20,4},{24,8},{28,12},{1,17},{... | collective-permute-start | bytes 98312 | tf_op jit(solution)/shard_map/ppermute | solution.py:576
  33.1 4.8 %collective-permute-start.10 = (bf16[32,512]{1,0:T(8,128)(2,1)S(1)}, bf16[32,512]{1,0:T(8,128)(2,1)S(1)}, u32[]{:S(2)}, u32[]{:S(2)}) collective-permute-start(bf16[32,512]{1,0:T(8,128)(2,1)S(1)} %recur.1.own_ref), channel_id=1, source_target_pairs={{0,8},{4,12},{8,0},{12,4},{16,24},{20,28},{24,16},{28,20},{1,9},{5... | collective-permute-start | bytes 98312 | tf_op jit(solution)/shard_map/ppermute | solution.py:576
  38.3 1.4 %collective-permute-start.13 = (bf16[512,128]{1,0:T(8,128)(2,1)S(1)}, bf16[512,128]{1,0:T(8,128)(2,1)S(1)}, u32[]{:S(2)}, u32[]{:S(2)}) collective-permute-start(bf16[512,128]{1,0:T(8,128)(2,1)S(1)} %get-tuple-element.47), channel_id=1, source_target_pairs={{0,1},{1,0},{2,3},{3,2},{4,5},{5,4},{6,7},{7,6},{8,9},{9,8},{10,11... | collective-permute-start | bytes 393224 | tf_op jit(solution)/shard_map/ppermute | solution.py:571
  39.7 4.9 %collective-permute-start.14 = (bf16[128,128]{1,0:T(8,128)(2,1)S(1)}, bf16[128,128]{1,0:T(8,128)(2,1)S(1)}, u32[]{:S(2)}, u32[]{:S(2)}) collective-permute-start(bf16[128,128]{1,0:T(8,128)(2,1)S(1)} %get-tuple-element.49), channel_id=1, source_target_pairs={{0,2},{1,3},{2,0},{3,1},{4,6},{5,7},{6,4},{7,5},{8,10},{9,11},{10,... | collective-permute-start | bytes 98312 | tf_op jit(solution)/shard_map/ppermute | solution.py:567
  41.3 3.9 %collective-permute-start.15 = (bf16[128,128]{1,0:T(8,128)(2,1)S(1)}, bf16[128,128]{1,0:T(8,128)(2,1)S(1)}, u32[]{:S(2)}, u32[]{:S(2)}) collective-permute-start(bf16[128,128]{1,0:T(8,128)(2,1)S(1)} %get-tuple-element.50), channel_id=1, source_target_pairs={{0,4},{1,5},{2,6},{3,7},{4,0},{5,1},{6,2},{7,3},{8,12},{9,13},{10,... | collective-permute-start | bytes 98312 | tf_op jit(solution)/shard_map/ppermute | solution.py:567
  42.8 4.8 %collective-permute-start.16 = (bf16[128,128]{1,0:T(8,128)(2,1)S(1)}, bf16[128,128]{1,0:T(8,128)(2,1)S(1)}, u32[]{:S(2)}, u32[]{:S(2)}) collective-permute-start(bf16[128,128]{1,0:T(8,128)(2,1)S(1)} %get-tuple-element.51), channel_id=1, source_target_pairs={{0,6},{1,7},{2,4},{3,5},{4,2},{5,3},{6,0},{7,1},{8,14},{9,15},{10,... | collective-permute-start | bytes 98312 | tf_op jit(solution)/shard_map/ppermute | solution.py:567
where the time goes:
time: 48.5 us; the launch traced here: 48.3 us
  starting transfers between devices  23.2 us (48%)
  waiting for transfers between devices  15.5 us (32%)
  Pallas kernels  8.79 us (18%)
  between operations  0.78 us (2%)
    ppermute x9, starting transfers between devices, along(): lax.ppermute(x, 'kv', [(s, PAIR * target(s // PAIR, k, count) + s % PAIR)...  13.8 us
    ppermute x9, waiting for transfers between devices, along(): lax.ppermute(x, 'kv', [(s, PAIR * target(s // PAIR, k, count) + s % PAIR)...  8.16 us
    ppermute x5, starting transfers between devices, swap(): lax.ppermute(x, axis, [(s, s - s % PAIR + (s + 1) % PAIR) for s in range(...  5.79 us
    ppermute x5, waiting for transfers between devices, swap(): lax.ppermute(x, axis, [(s, s - s % PAIR + (s + 1) % PAIR) for s in range(...  4.36 us
    ppermute x3, starting transfers between devices, across_groups(): return lax.ppermute(x, ('kv', 'tp'), moves)  3.55 us
    pallas_call x2, Pallas kernels, fold(): pl.pallas_call(functools.partial(fold_kernel, start), out_shape=[jax.Shap...  3.42 us
    ppermute x3, waiting for transfers between devices, across_groups(): return lax.ppermute(x, ('kv', 'tp'), moves)  2.95 us
    pallas_call x1, Pallas kernels, project(): pl.pallas_call(functools.partial(project_kernel, outer), out_shape=shapes...  2.24 us
  transfers between devices with their start and end apart: 17, of which 9 were waited for; matrix products, arithmetic and copies ran while one was open for 0% of the time, Pallas kernels for 11%

commit v1 on v0

--- a/solution.py
+++ b/solution.py
@@ -62,97 +62,112 @@
     return high, (x - high.astype(f32)).astype(bf16)
 
 
-def project_kernel(outer, x_hbm, gain_hbm, wq_hbm, wf_hbm, wv_hbm, *rest):
-    across_ref, stay_ref, squares_ref, own_ref = rest[:4]
-    ahead = rest[4 : 3 + outer]
-    x_ref, gain_ref, w_ref, terms_ref, sems = rest[3 + outer :]
+def project_kernel(outer, x_hbm, gain_hbm, wf_hbm, wv_hbm, *rest):
+    across_ref, stay_ref, squares_ref, scaled_ref, x_ref, gain_ref, w_ref, sems = rest
     tokens, features = x_ref.shape
-    cols = wq_hbm.shape[1]
+    cols = wf_hbm.shape[1]
     blocks = cols // LANES
     local = tokens // (outer * PAIR)
     copies = [
         pltpu.make_async_copy(x_hbm, x_ref, sems.at[0]),
         pltpu.make_async_copy(gain_hbm, gain_ref, sems.at[1]),
     ]
-    for j, w in enumerate((wf_hbm, wv_hbm, wq_hbm)):
+    for j, w in enumerate((wf_hbm, wv_hbm)):
         copies.append(pltpu.make_async_copy(w, w_ref.at[j], sems.at[2 + j]))
     for c in copies:
         c.start()
-    copies[0].wait()
-    copies[1].wait()
-    wide = x_ref[...].astype(f32)
-    scaled = (wide * gain_ref[...].astype(f32).reshape(1, features)).astype(bf16)
     me = lax.axis_index("kv")
     mine = lax.rem(me, PAIR)
     here = me // PAIR
-    nears, fars = [], []
+    copies[0].wait()
+    copies[1].wait()
+    gain = gain_ref[...].astype(f32).reshape(1, features)
     for k in range(outer):
         there = target(here, k, outer) * PAIR
-        nears.append(pl.ds(pl.multiple_of((there + mine) * local, PACK), local))
-        fars.append(pl.ds(pl.multiple_of((there + 1 - mine) * local, PACK), local))
-    for j in range(3):
+        for r, side in enumerate((mine, 1 - mine)):
+            block = x_ref[pl.ds(pl.multiple_of((there + side) * local, PACK), local), :]
+            at = pl.ds((k * PAIR + r) * local, local)
+            scaled_ref[at, :] = (block.astype(f32) * gain).astype(bf16)
+    wide = x_ref[...].astype(f32)
+    squares = wide * wide
+    folded = squares[:, :LANES]
+    for b in range(1, features // LANES):
+        folded = folded + squares[:, b * LANES : (b + 1) * LANES]
+    row = jnp.sum(folded.T, axis=0, keepdims=True)
+    spread = jnp.concatenate(
+        [row[:, r * LANES : (r + 1) * LANES] for r in range(square_rows(tokens))], axis=0
+    )
+    squares_ref[...] = spread
+    across_ref[outer * 2 * blocks * local :, :] = coded(spread)
+    for j in range(2):
         copies[2 + j].wait()
-        terms = jnp.dot(scaled, w_ref[j], preferred_element_type=f32)
-        for b in range(blocks):
-            terms_ref[j * blocks + b] = terms[:, b * LANES : (b + 1) * LANES]
-        if j == 2:
-            break
+        terms = jnp.dot(scaled_ref[...], w_ref[j], preferred_element_type=f32)
         for k in range(outer):
-            for b in range(j * blocks, (j + 1) * blocks):
-                at = pl.ds((k * 2 * blocks + b) * local, local)
-                stay_ref[at, :] = terms_ref[b, nears[k], :]
-                across_ref[at, :] = terms_ref[b, fars[k], :].astype(bf16)
-        if j == 0:
-            squares = wide * wide
-            folded = squares[:, :LANES]
-            for b in range(1, features // LANES):
-                folded = folded + squares[:, b * LANES : (b + 1) * LANES]
-            row = jnp.sum(folded.T, axis=0, keepdims=True)
-            rows = square_rows(tokens)
-            spread = jnp.concatenate(
-                [row[:, r * LANES : (r + 1) * LANES] for r in range(rows)], axis=0
-            )
-            squares_ref[...] = spread
-            across_ref[outer * 2 * blocks * local :, :] = coded(spread)
-    for k in range(outer):
-        for b in range(blocks):
-            for r, which in enumerate((nears[k], fars[k])):
-                at = pl.ds((r * blocks + b) * local, local)
-                piece = terms_ref[2 * blocks + b, which, :]
-                if k:
-                    ahead[k - 1][at, :] = piece.astype(bf16)
-                else:
-                    own_ref[at, :] = piece
-
-
-def project(inputs, norm_gain, w_query, w_forget, w_value, outer):
+            start = k * PAIR * local
+            for b in range(blocks):
+                at = pl.ds((k * 2 * blocks + j * blocks + b) * local, local)
+                part = terms[start : start + PAIR * local, b * LANES : (b + 1) * LANES]
+                stay_ref[at, :] = part[:local]
+                across_ref[at, :] = part[local:].astype(bf16)
+
+
+def project(inputs, norm_gain, w_forget, w_value, outer):
     tokens, features = inputs.shape
-    cols = w_query.shape[1]
-    blocks = cols // LANES
-    local = tokens // (outer * PAIR)
-    section = 2 * blocks * local
-    shapes = [
-        jax.ShapeDtypeStruct((outer * section + coded_rows(tokens), LANES), bf16),
-        jax.ShapeDtypeStruct((outer * section, LANES), f32),
-        jax.ShapeDtypeStruct((square_rows(tokens), LANES), f32),
-        jax.ShapeDtypeStruct((section, LANES), f32),
-    ] + [jax.ShapeDtypeStruct((section, LANES), bf16)] * (outer - 1)
-    out = pl.pallas_call(
+    cols = w_forget.shape[1]
+    section = 2 * cols // LANES * tokens // (outer * PAIR)
+    return pl.pallas_call(
         functools.partial(project_kernel, outer),
-        out_shape=shapes,
-        in_specs=[pl.BlockSpec(memory_space=pltpu.HBM)] * 5,
-        out_specs=[WHOLE] * len(shapes),
+        out_shape=[
+            jax.ShapeDtypeStruct((outer * section + coded_rows(tokens), LANES), bf16),
+            jax.ShapeDtypeStruct((outer * section, LANES), f32),
+            jax.ShapeDtypeStruct((square_rows(tokens), LANES), f32),
+            jax.ShapeDtypeStruct((tokens, features), bf16),
+        ],
+        in_specs=[pl.BlockSpec(memory_space=pltpu.HBM)] * 4,
+        out_specs=[WHOLE] * 4,
         scratch_shapes=[
             VMEM((tokens, features), bf16),
             VMEM((features,), bf16),
-            VMEM((3, features, cols), bf16),
-            VMEM((3 * blocks, tokens, LANES), f32),
-            pltpu.SemaphoreType.DMA((5,)),
+            VMEM((2, features, cols), bf16),
+            pltpu.SemaphoreType.DMA((4,)),
         ],
+        cost_estimate=pl.CostEstimate(
+            flops=2_000_000_000, bytes_accessed=4 * features * cols, transcendentals=0
+        ),
         compiler_params=grant(24),
         name="project",
-    )(*in_hbm(inputs, norm_gain, w_query, w_forget, w_value))
-    return out[0], out[1], out[2], out[3], out[4:]
+    )(*in_hbm(inputs, norm_gain, w_forget, w_value))
+
+
+def query_kernel(outer, scaled_ref, w_ref, own_ref, *ahead):
+    local = scaled_ref.shape[0] // (outer * PAIR)
+    blocks = w_ref.shape[1] // LANES
+    terms = jnp.dot(scaled_ref[...], w_ref[...], preferred_element_type=f32)
+    for k in range(outer):
+        for r in range(PAIR):
+            start = (k * PAIR + r) * local
+            for b in range(blocks):
+                at = pl.ds((r * blocks + b) * local, local)
+                part = terms[start : start + local, b * LANES : (b + 1) * LANES]
+                if k:
+                    ahead[k - 1][at, :] = part.astype(bf16)
+                else:
+                    own_ref[at, :] = part
+
+
+def query(scaled, w_query, outer):
+    cols = w_query.shape[1]
+    section = 2 * cols // LANES * scaled.shape[0] // (outer * PAIR)
+    out = pl.pallas_call(
+        functools.partial(query_kernel, outer),
+        out_shape=[jax.ShapeDtypeStruct((section, LANES), f32)]
+        + [jax.ShapeDtypeStruct((section, LANES), bf16)] * (outer - 1),
+        in_specs=[WHOLE] * 2,
+        out_specs=[WHOLE] * outer,
+        compiler_params=grant(16),
+        name="query",
+    )(scaled, w_query)
+    return out[0], out[1:]
 
 
 def combine_kernel(outer, after_ref, *refs):
@@ -597,10 +612,9 @@
     width = inputs.shape[1] * parts
     outer = parts // PAIR
     order = far_first(outer)
-    across, stay, squares, own, ahead = project(
-        inputs, norm_gain, w_query, w_forget, w_value, outer
-    )
+    across, stay, squares, scaled = project(inputs, norm_gain, w_forget, w_value, outer)
     across = swap(across, "kv", parts)
+    own, ahead = query(scaled, w_query, outer)
     moved = []
     for k in order:
         moved.append(along(ahead[k - 1], k, parts))

time: 48.5 us -> 48.1 us (level)
    pallas_call x1 -> x2, Pallas kernels: 2.24 us -> 2.16 us  [the longest x1 1.86 us: project(): pl.pallas_call(functools.partial(project_kernel, outer), out_shape=[jax.S...]
  transfers between devices with their start and end apart: 17 -> 17, of which waited for: 9 -> 9; matrix products, arithmetic and copies ran while one was open for 0% -> 0% of each run, Pallas kernels for 11% -> 12%
where the time goes in v1:
time: 48.1 us; the launch traced here: 47.9 us
  starting transfers between devices  23.2 us (48%)
  waiting for transfers between devices  15.1 us (31%)
  Pallas kernels  8.71 us (18%)
  between operations  0.79 us (2%)
    ppermute x9, starting transfers between devices, along(): lax.ppermute(x, 'kv', [(s, PAIR * target(s // PAIR, k, count) + s % PAIR)...  13.9 us
    ppermute x9, waiting for transfers between devices, along(): lax.ppermute(x, 'kv', [(s, PAIR * target(s // PAIR, k, count) + s % PAIR)...  8.16 us
    ppermute x5, starting transfers between devices, swap(): lax.ppermute(x, axis, [(s, s - s % PAIR + (s + 1) % PAIR) for s in range(...  5.8 us
    ppermute x5, waiting for transfers between devices, swap(): lax.ppermute(x, axis, [(s, s - s % PAIR + (s + 1) % PAIR) for s in range(...  4 us
    ppermute x3, starting transfers between devices, across_groups(): return lax.ppermute(x, ('kv', 'tp'), moves)  3.55 us
    pallas_call x2, Pallas kernels, fold(): pl.pallas_call(functools.partial(fold_kernel, start), out_shape=[jax.Shap...  3.42 us
    ppermute x3, waiting for transfers between devices, across_groups(): return lax.ppermute(x, ('kv', 'tp'), moves)  2.95 us
    pallas_call x1, Pallas kernels, project(): pl.pallas_call(functools.partial(project_kernel, outer), out_shape=[jax.S...  1.86 us
  transfers between devices with their start and end apart: 17, of which 9 were waited for; matrix products, arithmetic and copies ran while one was open for 0% of the time, Pallas kernels for 12%

profile of v1, /device:TPU:0, one launch (start us, length us, event | category | flops | bytes accessed | tf_op | source)
XLA Modules:
  0.0 47.9 jit_solution(9666108258684021159)
XLA Ops:
  0.6 0.0 copy-start.1
  0.6 0.0 copy-start
  0.7 1.9 %project.1 = (bf16[1032,128]{1,0:T(8,128)(2,1)S(1)}, f32[1024,128]{1,0:T(8,128)S(1)}, f32[2,128]{1,0:T(2,128)S(1)}, bf16[256,512]{1,0:T(8,128)(2,1)S(1)}) custom-call(bf16[256,512]{1,0:T(8,128)(2,1)} %x_hbm.1, bf16[512]{0:T(512)(128)(2,1)} %gain_hbm.1, bf16[512,512]{1,0:T(8,128)(2,1)} %wf_hbm.1, bf16[512,512]{1,0:T(8,128)(2,1)} %wv_hbm.1), custom_call_target="tpu_custom_call" | custom-call | flops 2000000000 | bytes 1048576 | tf_op jit(solution)/shard_map/project/pallas_call | solution.py:118
  2.5 3.1 %collective-permute-start = (bf16[1032,128]{1,0:T(8,128)(2,1)S(1)}, bf16[1032,128]{1,0:T(8,128)(2,1)S(1)}, u32[]{:S(2)}, u32[]{:S(2)}) collective-permute-start(bf16[1032,128]{1,0:T(8,128)(2,1)S(1)} %get-tuple-element.31), channel_id=1, source_target_pairs={{0,4},{4,0},{8,12},{12,8},{16,20},{20,16},{24,28},{28,24},{1,5},{5... | collective-permute-start | bytes 792584 | tf_op jit(solution)/shard_map/ppermute | solution.py:586
  5.6 0.0 copy-done.1
  5.6 0.3 query.1
  5.9 3.7 %collective-permute-start.1 = (bf16[256,128]{1,0:T(8,128)(2,1)S(1)}, bf16[256,128]{1,0:T(8,128)(2,1)S(1)}, u32[]{:S(2)}, u32[]{:S(2)}) collective-permute-start(bf16[256,128]{1,0:T(8,128)(2,1)S(1)} %get-tuple-element.35), channel_id=1, source_target_pairs={{0,24},{4,28},{8,16},{12,20},{16,8},{20,12},{24,0},{28,4},{1,25},{... | collective-permute-start | bytes 196616 | tf_op jit(solution)/shard_map/ppermute | solution.py:591
  9.6 0.0 copy-done
  9.6 0.6 %collective-permute-start.11 = (bf16[256,512]{1,0:T(8,128)(2,1)S(1)}, bf16[256,512]{1,0:T(8,128)(2,1)S(1)}, u32[]{:S(2)}, u32[]{:S(2)}) collective-permute-start(bf16[256,512]{1,0:T(8,128)(2,1)S(1)} %get-tuple-element.57), channel_id=1, source_target_pairs={{0,4},{4,0},{8,12},{12,8},{16,20},{20,16},{24,28},{28,24},{1,5},{5... | collective-permute-start | bytes 786440 | tf_op jit(solution)/shard_map/ppermute | solution.py:586
  10.2 1.5 %collective-permute-start.12 = (bf16[256,512]{1,0:T(8,128)(2,1)S(1)}, bf16[256,512]{1,0:T(8,128)(2,1)S(1)}, u32[]{:S(2)}, u32[]{:S(2)}) collective-permute-start(bf16[256,512]{1,0:T(8,128)(2,1)S(1)} %get-tuple-element.56), channel_id=1, source_target_pairs={{0,4},{4,0},{8,12},{12,8},{16,20},{20,16},{24,28},{28,24},{1,5},{5... | collective-permute-start | bytes 786440 | tf_op jit(solution)/shard_map/ppermute | solution.py:586
  11.7 0.0 collective-permute-start.2
  11.7 0.4 collective-permute-done.1.refs_4_
  12.1 0.4 collective-permute-start.3
  12.5 1.7 %fold.2 = (f32[4,4,128,128]{3,2,1,0:T(8,128)S(1)}, bf16[4,4,128,128]{3,2,1,0:T(8,128)(2,1)S(1)}, bf16[4,4,128,128]{3,2,1,0:T(8,128)(2,1)S(1)}) custom-call(s32[8]{0:T(128)} %accepted_hbm.3, f32[1024,128]{1,0:T(8,128)S(1)} %get-tuple-element.29.after_ref.refs_1_, f32[8,4,128,128]{3,2,1,0:T(8,128)} %state_hbm.3, f32[8,4,512]{2,1,0:T(4,128)} %gate_hbm.3, ...), custom_call_target="tpu_custom_call" | custom-call | flops 1000000000 | bytes 6291456 | tf_op jit(solution)/shard_map/fold/pallas_call | solution.py:289
  14.2 2.8 %collective-permute-done.2.refs_5_ = bf16[256,128]{1,0:T(8,128)(2,1)S(1)} collective-permute-done((bf16[256,128]{1,0:T(8,128)(2,1)S(1)}, bf16[256,128]{1,0:T(8,128)(2,1)S(1)}, u32[]{:S(2)}, u32[]{:S(2)}) %collective-permute-start.2) | collective-permute-done | bytes 65568 | tf_op jit(solution)/shard_map/ppermute | solution.py:591
  17.1 0.0 collective-permute-done.3.refs_6_
  17.1 0.0 collective-permute-done.refs_0_
  17.1 0.1 combine.1
  17.1 0.0 copy-start.2
  17.1 0.0 copy-start.3
  17.2 0.6 %collective-permute-start.4 = (bf16[128,128]{1,0:T(8,128)(2,1)S(1)}, bf16[128,128]{1,0:T(8,128)(2,1)S(1)}, u32[]{:S(2)}, u32[]{:S(2)}) collective-permute-start(bf16[128,128]{1,0:T(8,128)(2,1)S(1)} %get-tuple-element.41.after_ref), channel_id=1, source_target_pairs={{0,4},{4,0},{8,12},{12,8},{16,20},{20,16},{24,28},{28,24},{1,5},{5... | collective-permute-start | bytes 98312 | tf_op jit(solution)/shard_map/ppermute | solution.py:586
  17.7 3.5 %collective-permute-start.5 = (bf16[264,128]{1,0:T(8,128)(2,1)S(1)}, bf16[264,128]{1,0:T(8,128)(2,1)S(1)}, u32[]{:S(2)}, u32[]{:S(2)}) collective-permute-start(bf16[264,128]{1,0:T(8,128)(2,1)S(1)} %get-tuple-element.45), channel_id=1, source_target_pairs={{0,24},{4,28},{8,16},{12,20},{16,8},{20,12},{24,0},{28,4},{1,25},{... | collective-permute-start | bytes 202760 | tf_op jit(solution)/shard_map/ppermute | solution.py:591
  21.2 0.0 collective-permute-start.6
  21.2 2.7 %collective-permute-done.4.refs_3_ = bf16[128,128]{1,0:T(8,128)(2,1)S(1)} collective-permute-done((bf16[128,128]{1,0:T(8,128)(2,1)S(1)}, bf16[128,128]{1,0:T(8,128)(2,1)S(1)}, u32[]{:S(2)}, u32[]{:S(2)}) %collective-permute-start.4) | collective-permute-done | bytes 32800 | tf_op jit(solution)/shard_map/ppermute | solution.py:586
  23.9 1.8 %collective-permute-start.7 = (bf16[264,128]{1,0:T(8,128)(2,1)S(1)}, bf16[264,128]{1,0:T(8,128)(2,1)S(1)}, u32[]{:S(2)}, u32[]{:S(2)}) collective-permute-start(bf16[264,128]{1,0:T(8,128)(2,1)S(1)} %get-tuple-element.47), channel_id=1, source_target_pairs={{0,8},{4,12},{8,0},{12,4},{16,24},{20,28},{24,16},{28,20},{1,9},{5... | collective-permute-start | bytes 202760 | tf_op jit(solution)/shard_map/ppermute | solution.py:591
  25.7 1.7 %fold.3 = (f32[4,4,128,128]{3,2,1,0:T(8,128)S(1)}, bf16[4,4,128,128]{3,2,1,0:T(8,128)(2,1)S(1)}, bf16[4,4,128,128]{3,2,1,0:T(8,128)(2,1)S(1)}) custom-call(s32[8]{0:T(128)} %accepted_hbm.3, bf16[128,128]{1,0:T(8,128)(2,1)S(1)} %get-tuple-element.41.after_ref, f32[8,4,128,128]{3,2,1,0:T(8,128)} %state_hbm.3, f32[8,4,512]{2,1,0:T(4,128)} %gate_hbm.3, ...), custom_call_target="tpu_custom_call" | custom-call | flops 1000000000 | bytes 6291456 | tf_op jit(solution)/shard_map/fold/pallas_call | solution.py:289
  27.4 0.0 collective-permute-done.5.refs_8_
  27.4 0.0 collective-permute-done.6.refs_9_
  27.4 0.8 %collective-permute-done.7.refs_10_ = bf16[264,128]{1,0:T(8,128)(2,1)S(1)} collective-permute-done((bf16[264,128]{1,0:T(8,128)(2,1)S(1)}, bf16[264,128]{1,0:T(8,128)(2,1)S(1)}, u32[]{:S(2)}, u32[]{:S(2)}) %collective-permute-start.7) | collective-permute-done | bytes 67616 | tf_op jit(solution)/shard_map/ppermute | solution.py:591
  28.2 0.0 copy-done.2
  28.2 0.0 copy-done.3
  28.2 0.7 %recur.1.own_ref = bf16[32,512]{1,0:T(8,128)(2,1)S(1)} custom-call(f32[256,128]{1,0:T(8,128)S(1)} %get-tuple-element.38.refs_0_, f32[2,128]{1,0:T(2,128)S(1)} %get-tuple-element.39.refs_1_, f32[128,128]{1,0:T(8,128)S(1)} %get-tuple-element.40.refs_2_, bf16[128,128]{1,0:T(8,128)(2,1)S(1)} %collective-permute-done.4.refs_3_, ...), custom_call_target="tpu_custom_call" | custom-call | tf_op jit(solution)/shard_map/recur/pallas_call | solution.py:432
  28.8 3.9 %collective-permute-start.8 = (bf16[32,512]{1,0:T(8,128)(2,1)S(1)}, bf16[32,512]{1,0:T(8,128)(2,1)S(1)}, u32[]{:S(2)}, u32[]{:S(2)}) collective-permute-start(bf16[32,512]{1,0:T(8,128)(2,1)S(1)} %recur.1.own_ref), channel_id=1, source_target_pairs={{0,24},{4,28},{8,16},{12,20},{16,8},{20,12},{24,0},{28,4},{1,25},{... | collective-permute-start | bytes 98312 | tf_op jit(solution)/shard_map/ppermute | solution.py:591
  32.7 0.0 collective-permute-start.9
  32.7 0.6 %collective-permute-start.10 = (bf16[32,512]{1,0:T(8,128)(2,1)S(1)}, bf16[32,512]{1,0:T(8,128)(2,1)S(1)}, u32[]{:S(2)}, u32[]{:S(2)}) collective-permute-start(bf16[32,512]{1,0:T(8,128)(2,1)S(1)} %recur.1.own_ref), channel_id=1, source_target_pairs={{0,8},{4,12},{8,0},{12,4},{16,24},{20,28},{24,16},{28,20},{1,9},{5... | collective-permute-start | bytes 98312 | tf_op jit(solution)/shard_map/ppermute | solution.py:591
  33.4 1.4 %collective-permute-done.8.refs_0_ = bf16[32,512]{1,0:T(8,128)(2,1)S(1)} collective-permute-done((bf16[32,512]{1,0:T(8,128)(2,1)S(1)}, bf16[32,512]{1,0:T(8,128)(2,1)S(1)}, u32[]{:S(2)}, u32[]{:S(2)}) %collective-permute-start.8) | collective-permute-done | bytes 32800 | tf_op jit(solution)/shard_map/ppermute | solution.py:591
  34.7 2.8 %collective-permute-done.9.refs_1_ = bf16[32,512]{1,0:T(8,128)(2,1)S(1)} collective-permute-done((bf16[32,512]{1,0:T(8,128)(2,1)S(1)}, bf16[32,512]{1,0:T(8,128)(2,1)S(1)}, u32[]{:S(2)}, u32[]{:S(2)}) %collective-permute-start.9) | collective-permute-done | bytes 32800 | tf_op jit(solution)/shard_map/ppermute | solution.py:591
  37.5 0.0 collective-permute-done.10.refs_2_
  37.5 0.0 collective-permute-done.11.upper_ref
  37.6 0.0 collective-permute-done.12.lower_ref
  37.6 0.3 mix.1
  37.9 0.1 collective-permute-start.13
  38.0 1.3 %collective-permute-done.13.other_ref = bf16[512,128]{1,0:T(8,128)(2,1)S(1)} collective-permute-done((bf16[512,128]{1,0:T(8,128)(2,1)S(1)}, bf16[512,128]{1,0:T(8,128)(2,1)S(1)}, u32[]{:S(2)}, u32[]{:S(2)}) %collective-permute-start.13) | collective-permute-done | bytes 131104 | tf_op jit(solution)/shard_map/ppermute | solution.py:586
  39.4 1.6 %collective-permute-start.14 = (bf16[128,128]{1,0:T(8,128)(2,1)S(1)}, bf16[128,128]{1,0:T(8,128)(2,1)S(1)}, u32[]{:S(2)}, u32[]{:S(2)}) collective-permute-start(bf16[128,128]{1,0:T(8,128)(2,1)S(1)} %get-tuple-element.51), channel_id=1, source_target_pairs={{0,2},{1,3},{2,0},{3,1},{4,6},{5,7},{6,4},{7,5},{8,10},{9,11},{10,... | collective-permute-start | bytes 98312 | tf_op jit(solution)/shard_map/ppermute | solution.py:582
  40.9 1.5 %collective-permute-start.15 = (bf16[128,128]{1,0:T(8,128)(2,1)S(1)}, bf16[128,128]{1,0:T(8,128)(2,1)S(1)}, u32[]{:S(2)}, u32[]{:S(2)}) collective-permute-start(bf16[128,128]{1,0:T(8,128)(2,1)S(1)} %get-tuple-element.52), channel_id=1, source_target_pairs={{0,4},{1,5},{2,6},{3,7},{4,0},{5,1},{6,2},{7,3},{8,12},{9,13},{10,... | collective-permute-start | bytes 98312 | tf_op jit(solution)/shard_map/ppermute | solution.py:582
  42.4 0.5 collective-permute-start.16
  42.9 1.4 %store.1 = f32[8,4,128,128]{3,2,1,0:T(8,128)} custom-call(bf16[128,128]{1,0:T(8,128)(2,1)S(1)} %get-tuple-element.41.after_ref, f32[4,4,128,128]{3,2,1,0:T(8,128)S(1)} %get-tuple-element.54.refs_0_, f32[4,4,128,128]{3,2,1,0:T(8,128)S(1)} %get-tuple-element.55.refs_1_), custom_call_target="tpu_custom_call" | custom-call | flops 1000000000 | bytes 64 | tf_op jit(solution)/shard_map/store/pallas_call | solution.py:336
  44.3 0.0 collective-permute-done.14.refs_1_
  44.3 0.5 %collective-permute-done.15.refs_2_ = bf16[128,128]{1,0:T(8,128)(2,1)S(1)} collective-permute-done((bf16[128,128]{1,0:T(8,128)(2,1)S(1)}, bf16[128,128]{1,0:T(8,128)(2,1)S(1)}, u32[]{:S(2)}, u32[]{:S(2)}) %collective-permute-start.15) | collective-permute-done | bytes 32800 | tf_op jit(solution)/shard_map/ppermute | solution.py:582
  44.8 2.4 %collective-permute-done.16.refs_3_ = bf16[128,128]{1,0:T(8,128)(2,1)S(1)} collective-permute-done((bf16[128,128]{1,0:T(8,128)(2,1)S(1)}, bf16[128,128]{1,0:T(8,128)(2,1)S(1)}, u32[]{:S(2)}, u32[]{:S(2)}) %collective-permute-start.16) | collective-permute-done | bytes 32800 | tf_op jit(solution)/shard_map/ppermute | solution.py:582
  47.2 0.6 %finish.1 = bf16[256,128]{1,0:T(8,128)(2,1)} custom-call(f32[128,128]{1,0:T(8,128)S(1)} %get-tuple-element.50.refs_0_, bf16[128,128]{1,0:T(8,128)(2,1)S(1)} %collective-permute-done.14.refs_1_, bf16[128,128]{1,0:T(8,128)(2,1)S(1)} %collective-permute-done.15.refs_2_, bf16[128,128]{1,0:T(8,128)(2,1)S(1)} %collective-permute-done.16.refs_3_), custom_call_target="tpu_custom_call" | custom-call | tf_op jit(solution)/shard_map/finish/pallas_call | solution.py:552
  (3 shorter events, 0.1 us)
Async XLA Ops:
  0.6 5.0 %copy-start.1 = (bf16[512,512]{1,0:T(8,128)(2,1)S(1)}, bf16[512,512]{1,0:T(8,128)(2,1)}, u32[]{:S(2)}) copy-start(bf16[512,512]{1,0:T(8,128)(2,1)} %w_ref.1) | copy-start | bytes 1572868
  0.6 8.9 %copy-start = (bf16[512,512]{1,0:T(8,128)(2,1)S(1)}, bf16[512,512]{1,0:T(8,128)(2,1)}, u32[]{:S(2)}) copy-start(bf16[512,512]{1,0:T(8,128)(2,1)} %near_w_ref.1) | copy-start | bytes 1572868
  2.5 14.5 %collective-permute-start = (bf16[1032,128]{1,0:T(8,128)(2,1)S(1)}, bf16[1032,128]{1,0:T(8,128)(2,1)S(1)}, u32[]{:S(2)}, u32[]{:S(2)}) collective-permute-start(bf16[1032,128]{1,0:T(8,128)(2,1)S(1)} %get-tuple-element.31), channel_id=1, source_target_pairs={{0,4},{4,0},{8,12},{12,8},{16,20},{20,16},{24,28},{28,24},{1,5},{5... | collective-permute-start | bytes 792584 | tf_op jit(solution)/shard_map/ppermute | solution.py:586
  5.9 6.2 %collective-permute-start.1 = (bf16[256,128]{1,0:T(8,128)(2,1)S(1)}, bf16[256,128]{1,0:T(8,128)(2,1)S(1)}, u32[]{:S(2)}, u32[]{:S(2)}) collective-permute-start(bf16[256,128]{1,0:T(8,128)(2,1)S(1)} %get-tuple-element.35), channel_id=1, source_target_pairs={{0,24},{4,28},{8,16},{12,20},{16,8},{20,12},{24,0},{28,4},{1,25},{... | collective-permute-start | bytes 196616 | tf_op jit(solution)/shard_map/ppermute | solution.py:591
  9.6 28.0 %collective-permute-start.11 = (bf16[256,512]{1,0:T(8,128)(2,1)S(1)}, bf16[256,512]{1,0:T(8,128)(2,1)S(1)}, u32[]{:S(2)}, u32[]{:S(2)}) collective-permute-start(bf16[256,512]{1,0:T(8,128)(2,1)S(1)} %get-tuple-element.57), channel_id=1, source_target_pairs={{0,4},{4,0},{8,12},{12,8},{16,20},{20,16},{24,28},{28,24},{1,5},{5... | collective-permute-start | bytes 786440 | tf_op jit(solution)/shard_map/ppermute | solution.py:586
  10.2 27.4 %collective-permute-start.12 = (bf16[256,512]{1,0:T(8,128)(2,1)S(1)}, bf16[256,512]{1,0:T(8,128)(2,1)S(1)}, u32[]{:S(2)}, u32[]{:S(2)}) collective-permute-start(bf16[256,512]{1,0:T(8,128)(2,1)S(1)} %get-tuple-element.56), channel_id=1, source_target_pairs={{0,4},{4,0},{8,12},{12,8},{16,20},{20,16},{24,28},{28,24},{1,5},{5... | collective-permute-start | bytes 786440 | tf_op jit(solution)/shard_map/ppermute | solution.py:586
  11.7 5.4 %collective-permute-start.2 = (bf16[256,128]{1,0:T(8,128)(2,1)S(1)}, bf16[256,128]{1,0:T(8,128)(2,1)S(1)}, u32[]{:S(2)}, u32[]{:S(2)}) collective-permute-start(bf16[256,128]{1,0:T(8,128)(2,1)S(1)} %get-tuple-element.36), channel_id=1, source_target_pairs={{0,16},{4,20},{8,24},{12,28},{16,0},{20,4},{24,8},{28,12},{1,17},{... | collective-permute-start | bytes 196616 | tf_op jit(solution)/shard_map/ppermute | solution.py:591
  12.1 5.0 %collective-permute-start.3 = (bf16[256,128]{1,0:T(8,128)(2,1)S(1)}, bf16[256,128]{1,0:T(8,128)(2,1)S(1)}, u32[]{:S(2)}, u32[]{:S(2)}) collective-permute-start(bf16[256,128]{1,0:T(8,128)(2,1)S(1)} %get-tuple-element.37), channel_id=1, source_target_pairs={{0,8},{4,12},{8,0},{12,4},{16,24},{20,28},{24,16},{28,20},{1,9},{5... | collective-permute-start | bytes 196616 | tf_op jit(solution)/shard_map/ppermute | solution.py:591
  17.1 11.0 %copy-start.2 = (f32[512]{0:T(512)S(1)}, f32[512]{0:T(512)}, u32[]{:S(2)}) copy-start(f32[512]{0:T(512)} %param.17) | copy-start | bytes 6148
  17.1 11.0 %copy-start.3 = (f32[512]{0:T(512)S(1)}, f32[512]{0:T(512)}, u32[]{:S(2)}) copy-start(f32[512]{0:T(512)} %param.18) | copy-start | bytes 6148
  17.2 6.7 %collective-permute-start.4 = (bf16[128,128]{1,0:T(8,128)(2,1)S(1)}, bf16[128,128]{1,0:T(8,128)(2,1)S(1)}, u32[]{:S(2)}, u32[]{:S(2)}) collective-permute-start(bf16[128,128]{1,0:T(8,128)(2,1)S(1)} %get-tuple-element.41.after_ref), channel_id=1, source_target_pairs={{0,4},{4,0},{8,12},{12,8},{16,20},{20,16},{24,28},{28,24},{1,5},{5... | collective-permute-start | bytes 98312 | tf_op jit(solution)/shard_map/ppermute | solution.py:586
  17.7 9.6 %collective-permute-start.5 = (bf16[264,128]{1,0:T(8,128)(2,1)S(1)}, bf16[264,128]{1,0:T(8,128)(2,1)S(1)}, u32[]{:S(2)}, u32[]{:S(2)}) collective-permute-start(bf16[264,128]{1,0:T(8,128)(2,1)S(1)} %get-tuple-element.45), channel_id=1, source_target_pairs={{0,24},{4,28},{8,16},{12,20},{16,8},{20,12},{24,0},{28,4},{1,25},{... | collective-permute-start | bytes 202760 | tf_op jit(solution)/shard_map/ppermute | solution.py:591
  21.2 6.2 %collective-permute-start.6 = (bf16[264,128]{1,0:T(8,128)(2,1)S(1)}, bf16[264,128]{1,0:T(8,128)(2,1)S(1)}, u32[]{:S(2)}, u32[]{:S(2)}) collective-permute-start(bf16[264,128]{1,0:T(8,128)(2,1)S(1)} %get-tuple-element.46), channel_id=1, source_target_pairs={{0,16},{4,20},{8,24},{12,28},{16,0},{20,4},{24,8},{28,12},{1,17},{... | collective-permute-start | bytes 202760 | tf_op jit(solution)/shard_map/ppermute | solution.py:591
  23.9 4.3 %collective-permute-start.7 = (bf16[264,128]{1,0:T(8,128)(2,1)S(1)}, bf16[264,128]{1,0:T(8,128)(2,1)S(1)}, u32[]{:S(2)}, u32[]{:S(2)}) collective-permute-start(bf16[264,128]{1,0:T(8,128)(2,1)S(1)} %get-tuple-element.47), channel_id=1, source_target_pairs={{0,8},{4,12},{8,0},{12,4},{16,24},{20,28},{24,16},{28,20},{1,9},{5... | collective-permute-start | bytes 202760 | tf_op jit(solution)/shard_map/ppermute | solution.py:591
  28.8 5.9 %collective-permute-start.8 = (bf16[32,512]{1,0:T(8,128)(2,1)S(1)}, bf16[32,512]{1,0:T(8,128)(2,1)S(1)}, u32[]{:S(2)}, u32[]{:S(2)}) collective-permute-start(bf16[32,512]{1,0:T(8,128)(2,1)S(1)} %recur.1.own_ref), channel_id=1, source_target_pairs={{0,24},{4,28},{8,16},{12,20},{16,8},{20,12},{24,0},{28,4},{1,25},{... | collective-permute-start | bytes 98312 | tf_op jit(solution)/shard_map/ppermute | solution.py:591
  32.7 4.8 %collective-permute-start.9 = (bf16[32,512]{1,0:T(8,128)(2,1)S(1)}, bf16[32,512]{1,0:T(8,128)(2,1)S(1)}, u32[]{:S(2)}, u32[]{:S(2)}) collective-permute-start(bf16[32,512]{1,0:T(8,128)(2,1)S(1)} %recur.1.own_ref), channel_id=1, source_target_pairs={{0,16},{4,20},{8,24},{12,28},{16,0},{20,4},{24,8},{28,12},{1,17},{... | collective-permute-start | bytes 98312 | tf_op jit(solution)/shard_map/ppermute | solution.py:591
  32.7 4.8 %collective-permute-start.10 = (bf16[32,512]{1,0:T(8,128)(2,1)S(1)}, bf16[32,512]{1,0:T(8,128)(2,1)S(1)}, u32[]{:S(2)}, u32[]{:S(2)}) collective-permute-start(bf16[32,512]{1,0:T(8,128)(2,1)S(1)} %recur.1.own_ref), channel_id=1, source_target_pairs={{0,8},{4,12},{8,0},{12,4},{16,24},{20,28},{24,16},{28,20},{1,9},{5... | collective-permute-start | bytes 98312 | tf_op jit(solution)/shard_map/ppermute | solution.py:591
  37.9 1.4 %collective-permute-start.13 = (bf16[512,128]{1,0:T(8,128)(2,1)S(1)}, bf16[512,128]{1,0:T(8,128)(2,1)S(1)}, u32[]{:S(2)}, u32[]{:S(2)}) collective-permute-start(bf16[512,128]{1,0:T(8,128)(2,1)S(1)} %get-tuple-element.49), channel_id=1, source_target_pairs={{0,1},{1,0},{2,3},{3,2},{4,5},{5,4},{6,7},{7,6},{8,9},{9,8},{10,11... | collective-permute-start | bytes 393224 | tf_op jit(solution)/shard_map/ppermute | solution.py:586
  39.4 4.9 %collective-permute-start.14 = (bf16[128,128]{1,0:T(8,128)(2,1)S(1)}, bf16[128,128]{1,0:T(8,128)(2,1)S(1)}, u32[]{:S(2)}, u32[]{:S(2)}) collective-permute-start(bf16[128,128]{1,0:T(8,128)(2,1)S(1)} %get-tuple-element.51), channel_id=1, source_target_pairs={{0,2},{1,3},{2,0},{3,1},{4,6},{5,7},{6,4},{7,5},{8,10},{9,11},{10,... | collective-permute-start | bytes 98312 | tf_op jit(solution)/shard_map/ppermute | solution.py:582
  40.9 3.9 %collective-permute-start.15 = (bf16[128,128]{1,0:T(8,128)(2,1)S(1)}, bf16[128,128]{1,0:T(8,128)(2,1)S(1)}, u32[]{:S(2)}, u32[]{:S(2)}) collective-permute-start(bf16[128,128]{1,0:T(8,128)(2,1)S(1)} %get-tuple-element.52), channel_id=1, source_target_pairs={{0,4},{1,5},{2,6},{3,7},{4,0},{5,1},{6,2},{7,3},{8,12},{9,13},{10,... | collective-permute-start | bytes 98312 | tf_op jit(solution)/shard_map/ppermute | solution.py:582
  42.4 4.8 %collective-permute-start.16 = (bf16[128,128]{1,0:T(8,128)(2,1)S(1)}, bf16[128,128]{1,0:T(8,128)(2,1)S(1)}, u32[]{:S(2)}, u32[]{:S(2)}) collective-permute-start(bf16[128,128]{1,0:T(8,128)(2,1)S(1)} %get-tuple-element.53), channel_id=1, source_target_pairs={{0,6},{1,7},{2,4},{3,5},{4,2},{5,3},{6,0},{7,1},{8,14},{9,15},{10,... | collective-permute-start | bytes 98312 | tf_op jit(solution)/shard_map/ppermute | solution.py:582

commit v2 on v1

--- a/solution.py
+++ b/solution.py
@@ -486,8 +486,9 @@
         for k in range(half):
             group = target(me // PAIR, k, half) * PAIR
             at = pl.ds((side * half + k) * height, height)
-            keep_ref[at, :] = cols_ref[side, group + mine]
-            send_ref[at, :] = cols_ref[side, group + 1 - mine].astype(bf16)
+            member = 1 - mine if side or k else mine
+            keep_ref[at, :] = cols_ref[side, group + member]
+            send_ref[at, :] = cols_ref[side, group + 1 - member].astype(bf16)
 
 
 def mix(own, others, near_w, upper, lower, groups):
@@ -571,13 +572,12 @@
     return sorted(range(1, count), key=lambda k: -k)
 
 
-def across_groups(x, k, groups, parts, other):
-    half = groups // PAIR
+def cross(x, parts, groups, pair=0, outer=0, half=0, member=1):
     moves = []
     for s in range(parts):
-        to = s - s % PAIR + (s + other) % PAIR
+        to = target(s // PAIR, outer, parts // PAIR) * PAIR + (s + pair) % PAIR
         for g in range(groups):
-            there = target(g // PAIR, k, half) * PAIR + g % PAIR
+            there = target(g // PAIR, half, groups // PAIR) * PAIR + (g + member) % PAIR
             moves.append((s * groups + g, to * groups + there))
     return lax.ppermute(x, ("kv", "tp"), moves)
 
@@ -657,7 +657,7 @@
     half = groups // PAIR
     pieces = [own] + [None] * (groups - 1)
     for i in reversed(range(1, groups)):
-        pieces[i] = across_groups(sends[i - 1], i % half, groups, parts, i // half)
+        pieces[i] = cross(sends[i - 1], parts, groups, pair=i // half, half=i % half)
     return finish(pieces, outer), base_state
 
 

time: 48.1 us -> 47.2 us (0.981)
  starting transfers between devices: 23.2 us -> 22.7 us
    ppermute x3, starting transfers between devices: 3.55 us -> 3.03 us  [cross(): return lax.ppermute(x, ('kv', 'tp'), moves)]
where the time goes in v2:
time: 47.2 us; the launch traced here: 47.1 us
  starting transfers between devices  22.7 us (48%)
  waiting for transfers between devices  14.8 us (31%)
  Pallas kernels  8.71 us (18%)
  between operations  0.79 us (2%)
    ppermute x9, starting transfers between devices, along(): lax.ppermute(x, 'kv', [(s, PAIR * target(s // PAIR, k, count) + s % PAIR)...  13.9 us
    ppermute x9, waiting for transfers between devices, along(): lax.ppermute(x, 'kv', [(s, PAIR * target(s // PAIR, k, count) + s % PAIR)...  8.16 us
    ppermute x5, starting transfers between devices, swap(): lax.ppermute(x, axis, [(s, s - s % PAIR + (s + 1) % PAIR) for s in range(...  5.8 us
    ppermute x5, waiting for transfers between devices, swap(): lax.ppermute(x, axis, [(s, s - s % PAIR + (s + 1) % PAIR) for s in range(...  4 us
    pallas_call x2, Pallas kernels, fold(): pl.pallas_call(functools.partial(fold_kernel, start), out_shape=[jax.Shap...  3.42 us
    ppermute x3, starting transfers between devices, cross(): return lax.ppermute(x, ('kv', 'tp'), moves)  3.03 us
    ppermute x3, waiting for transfers between devices, cross(): return lax.ppermute(x, ('kv', 'tp'), moves)  2.64 us
    pallas_call x1, Pallas kernels, project(): pl.pallas_call(functools.partial(project_kernel, outer), out_shape=[jax.S...  1.86 us
  transfers between devices with their start and end apart: 17, of which 9 were waited for; matrix products, arithmetic and copies ran while one was open for 0% of the time, Pallas kernels for 12%

profile of v2, /device:TPU:0, one launch (start us, length us, event | category | flops | bytes accessed | tf_op | source)
XLA Modules:
  0.0 47.1 jit_solution(10306811694857038280)
XLA Ops:
  0.6 0.0 copy-start.1
  0.6 0.0 copy-start
  0.7 1.9 %project.1 = (bf16[1032,128]{1,0:T(8,128)(2,1)S(1)}, f32[1024,128]{1,0:T(8,128)S(1)}, f32[2,128]{1,0:T(2,128)S(1)}, bf16[256,512]{1,0:T(8,128)(2,1)S(1)}) custom-call(bf16[256,512]{1,0:T(8,128)(2,1)} %x_hbm.1, bf16[512]{0:T(512)(128)(2,1)} %gain_hbm.1, bf16[512,512]{1,0:T(8,128)(2,1)} %wf_hbm.1, bf16[512,512]{1,0:T(8,128)(2,1)} %wv_hbm.1), custom_call_target="tpu_custom_call" | custom-call | flops 2000000000 | bytes 1048576 | tf_op jit(solution)/shard_map/project/pallas_call | solution.py:118
  2.5 3.1 %collective-permute-start = (bf16[1032,128]{1,0:T(8,128)(2,1)S(1)}, bf16[1032,128]{1,0:T(8,128)(2,1)S(1)}, u32[]{:S(2)}, u32[]{:S(2)}) collective-permute-start(bf16[1032,128]{1,0:T(8,128)(2,1)S(1)} %get-tuple-element.31), channel_id=1, source_target_pairs={{0,4},{4,0},{8,12},{12,8},{16,20},{20,16},{24,28},{28,24},{1,5},{5... | collective-permute-start | bytes 792584 | tf_op jit(solution)/shard_map/ppermute | solution.py:586
  5.6 0.0 copy-done.1
  5.6 0.3 query.1
  5.9 3.7 %collective-permute-start.1 = (bf16[256,128]{1,0:T(8,128)(2,1)S(1)}, bf16[256,128]{1,0:T(8,128)(2,1)S(1)}, u32[]{:S(2)}, u32[]{:S(2)}) collective-permute-start(bf16[256,128]{1,0:T(8,128)(2,1)S(1)} %get-tuple-element.35), channel_id=1, source_target_pairs={{0,24},{4,28},{8,16},{12,20},{16,8},{20,12},{24,0},{28,4},{1,25},{... | collective-permute-start | bytes 196616 | tf_op jit(solution)/shard_map/ppermute | solution.py:591
  9.6 0.0 copy-done
  9.6 0.6 %collective-permute-start.11 = (bf16[256,512]{1,0:T(8,128)(2,1)S(1)}, bf16[256,512]{1,0:T(8,128)(2,1)S(1)}, u32[]{:S(2)}, u32[]{:S(2)}) collective-permute-start(bf16[256,512]{1,0:T(8,128)(2,1)S(1)} %get-tuple-element.57), channel_id=1, source_target_pairs={{0,4},{4,0},{8,12},{12,8},{16,20},{20,16},{24,28},{28,24},{1,5},{5... | collective-permute-start | bytes 786440 | tf_op jit(solution)/shard_map/ppermute | solution.py:586
  10.2 1.5 %collective-permute-start.12 = (bf16[256,512]{1,0:T(8,128)(2,1)S(1)}, bf16[256,512]{1,0:T(8,128)(2,1)S(1)}, u32[]{:S(2)}, u32[]{:S(2)}) collective-permute-start(bf16[256,512]{1,0:T(8,128)(2,1)S(1)} %get-tuple-element.56), channel_id=1, source_target_pairs={{0,4},{4,0},{8,12},{12,8},{16,20},{20,16},{24,28},{28,24},{1,5},{5... | collective-permute-start | bytes 786440 | tf_op jit(solution)/shard_map/ppermute | solution.py:586
  11.7 0.0 collective-permute-start.2
  11.7 0.4 collective-permute-done.1.refs_4_
  12.1 0.4 collective-permute-start.3
  12.5 1.7 %fold.2 = (f32[4,4,128,128]{3,2,1,0:T(8,128)S(1)}, bf16[4,4,128,128]{3,2,1,0:T(8,128)(2,1)S(1)}, bf16[4,4,128,128]{3,2,1,0:T(8,128)(2,1)S(1)}) custom-call(s32[8]{0:T(128)} %accepted_hbm.3, f32[1024,128]{1,0:T(8,128)S(1)} %get-tuple-element.29.after_ref.refs_1_, f32[8,4,128,128]{3,2,1,0:T(8,128)} %state_hbm.3, f32[8,4,512]{2,1,0:T(4,128)} %gate_hbm.3, ...), custom_call_target="tpu_custom_call" | custom-call | flops 1000000000 | bytes 6291456 | tf_op jit(solution)/shard_map/fold/pallas_call | solution.py:289
  14.2 2.8 %collective-permute-done.2.refs_5_ = bf16[256,128]{1,0:T(8,128)(2,1)S(1)} collective-permute-done((bf16[256,128]{1,0:T(8,128)(2,1)S(1)}, bf16[256,128]{1,0:T(8,128)(2,1)S(1)}, u32[]{:S(2)}, u32[]{:S(2)}) %collective-permute-start.2) | collective-permute-done | bytes 65568 | tf_op jit(solution)/shard_map/ppermute | solution.py:591
  17.1 0.0 collective-permute-done.3.refs_6_
  17.1 0.0 collective-permute-done.refs_0_
  17.1 0.1 combine.1
  17.1 0.0 copy-start.2
  17.1 0.0 copy-start.3
  17.2 0.6 %collective-permute-start.4 = (bf16[128,128]{1,0:T(8,128)(2,1)S(1)}, bf16[128,128]{1,0:T(8,128)(2,1)S(1)}, u32[]{:S(2)}, u32[]{:S(2)}) collective-permute-start(bf16[128,128]{1,0:T(8,128)(2,1)S(1)} %get-tuple-element.41.after_ref), channel_id=1, source_target_pairs={{0,4},{4,0},{8,12},{12,8},{16,20},{20,16},{24,28},{28,24},{1,5},{5... | collective-permute-start | bytes 98312 | tf_op jit(solution)/shard_map/ppermute | solution.py:586
  17.7 3.5 %collective-permute-start.5 = (bf16[264,128]{1,0:T(8,128)(2,1)S(1)}, bf16[264,128]{1,0:T(8,128)(2,1)S(1)}, u32[]{:S(2)}, u32[]{:S(2)}) collective-permute-start(bf16[264,128]{1,0:T(8,128)(2,1)S(1)} %get-tuple-element.45), channel_id=1, source_target_pairs={{0,24},{4,28},{8,16},{12,20},{16,8},{20,12},{24,0},{28,4},{1,25},{... | collective-permute-start | bytes 202760 | tf_op jit(solution)/shard_map/ppermute | solution.py:591
  21.2 0.0 collective-permute-start.6
  21.2 2.7 %collective-permute-done.4.refs_3_ = bf16[128,128]{1,0:T(8,128)(2,1)S(1)} collective-permute-done((bf16[128,128]{1,0:T(8,128)(2,1)S(1)}, bf16[128,128]{1,0:T(8,128)(2,1)S(1)}, u32[]{:S(2)}, u32[]{:S(2)}) %collective-permute-start.4) | collective-permute-done | bytes 32800 | tf_op jit(solution)/shard_map/ppermute | solution.py:586
  23.9 1.8 %collective-permute-start.7 = (bf16[264,128]{1,0:T(8,128)(2,1)S(1)}, bf16[264,128]{1,0:T(8,128)(2,1)S(1)}, u32[]{:S(2)}, u32[]{:S(2)}) collective-permute-start(bf16[264,128]{1,0:T(8,128)(2,1)S(1)} %get-tuple-element.47), channel_id=1, source_target_pairs={{0,8},{4,12},{8,0},{12,4},{16,24},{20,28},{24,16},{28,20},{1,9},{5... | collective-permute-start | bytes 202760 | tf_op jit(solution)/shard_map/ppermute | solution.py:591
  25.7 1.7 %fold.3 = (f32[4,4,128,128]{3,2,1,0:T(8,128)S(1)}, bf16[4,4,128,128]{3,2,1,0:T(8,128)(2,1)S(1)}, bf16[4,4,128,128]{3,2,1,0:T(8,128)(2,1)S(1)}) custom-call(s32[8]{0:T(128)} %accepted_hbm.3, bf16[128,128]{1,0:T(8,128)(2,1)S(1)} %get-tuple-element.41.after_ref, f32[8,4,128,128]{3,2,1,0:T(8,128)} %state_hbm.3, f32[8,4,512]{2,1,0:T(4,128)} %gate_hbm.3, ...), custom_call_target="tpu_custom_call" | custom-call | flops 1000000000 | bytes 6291456 | tf_op jit(solution)/shard_map/fold/pallas_call | solution.py:289
  27.4 0.0 collective-permute-done.5.refs_8_
  27.4 0.0 collective-permute-done.6.refs_9_
  27.4 0.8 %collective-permute-done.7.refs_10_ = bf16[264,128]{1,0:T(8,128)(2,1)S(1)} collective-permute-done((bf16[264,128]{1,0:T(8,128)(2,1)S(1)}, bf16[264,128]{1,0:T(8,128)(2,1)S(1)}, u32[]{:S(2)}, u32[]{:S(2)}) %collective-permute-start.7) | collective-permute-done | bytes 67616 | tf_op jit(solution)/shard_map/ppermute | solution.py:591
  28.2 0.0 copy-done.2
  28.2 0.0 copy-done.3
  28.2 0.7 %recur.1.own_ref = bf16[32,512]{1,0:T(8,128)(2,1)S(1)} custom-call(f32[256,128]{1,0:T(8,128)S(1)} %get-tuple-element.38.refs_0_, f32[2,128]{1,0:T(2,128)S(1)} %get-tuple-element.39.refs_1_, f32[128,128]{1,0:T(8,128)S(1)} %get-tuple-element.40.refs_2_, bf16[128,128]{1,0:T(8,128)(2,1)S(1)} %collective-permute-done.4.refs_3_, ...), custom_call_target="tpu_custom_call" | custom-call | tf_op jit(solution)/shard_map/recur/pallas_call | solution.py:432
  28.8 3.9 %collective-permute-start.8 = (bf16[32,512]{1,0:T(8,128)(2,1)S(1)}, bf16[32,512]{1,0:T(8,128)(2,1)S(1)}, u32[]{:S(2)}, u32[]{:S(2)}) collective-permute-start(bf16[32,512]{1,0:T(8,128)(2,1)S(1)} %recur.1.own_ref), channel_id=1, source_target_pairs={{0,24},{4,28},{8,16},{12,20},{16,8},{20,12},{24,0},{28,4},{1,25},{... | collective-permute-start | bytes 98312 | tf_op jit(solution)/shard_map/ppermute | solution.py:591
  32.7 0.0 collective-permute-start.9
  32.7 0.6 %collective-permute-start.10 = (bf16[32,512]{1,0:T(8,128)(2,1)S(1)}, bf16[32,512]{1,0:T(8,128)(2,1)S(1)}, u32[]{:S(2)}, u32[]{:S(2)}) collective-permute-start(bf16[32,512]{1,0:T(8,128)(2,1)S(1)} %recur.1.own_ref), channel_id=1, source_target_pairs={{0,8},{4,12},{8,0},{12,4},{16,24},{20,28},{24,16},{28,20},{1,9},{5... | collective-permute-start | bytes 98312 | tf_op jit(solution)/shard_map/ppermute | solution.py:591
  33.4 1.4 %collective-permute-done.8.refs_0_ = bf16[32,512]{1,0:T(8,128)(2,1)S(1)} collective-permute-done((bf16[32,512]{1,0:T(8,128)(2,1)S(1)}, bf16[32,512]{1,0:T(8,128)(2,1)S(1)}, u32[]{:S(2)}, u32[]{:S(2)}) %collective-permute-start.8) | collective-permute-done | bytes 32800 | tf_op jit(solution)/shard_map/ppermute | solution.py:591
  34.7 2.8 %collective-permute-done.9.refs_1_ = bf16[32,512]{1,0:T(8,128)(2,1)S(1)} collective-permute-done((bf16[32,512]{1,0:T(8,128)(2,1)S(1)}, bf16[32,512]{1,0:T(8,128)(2,1)S(1)}, u32[]{:S(2)}, u32[]{:S(2)}) %collective-permute-start.9) | collective-permute-done | bytes 32800 | tf_op jit(solution)/shard_map/ppermute | solution.py:591
  37.5 0.0 collective-permute-done.10.refs_2_
  37.5 0.0 collective-permute-done.11.upper_ref
  37.6 0.0 collective-permute-done.12.lower_ref
  37.6 0.3 mix.1
  37.9 0.1 collective-permute-start.13
  38.0 1.3 %collective-permute-done.13.other_ref = bf16[512,128]{1,0:T(8,128)(2,1)S(1)} collective-permute-done((bf16[512,128]{1,0:T(8,128)(2,1)S(1)}, bf16[512,128]{1,0:T(8,128)(2,1)S(1)}, u32[]{:S(2)}, u32[]{:S(2)}) %collective-permute-start.13) | collective-permute-done | bytes 131104 | tf_op jit(solution)/shard_map/ppermute | solution.py:586
  39.4 1.3 %collective-permute-start.14 = (bf16[128,128]{1,0:T(8,128)(2,1)S(1)}, bf16[128,128]{1,0:T(8,128)(2,1)S(1)}, u32[]{:S(2)}, u32[]{:S(2)}) collective-permute-start(bf16[128,128]{1,0:T(8,128)(2,1)S(1)} %get-tuple-element.51), channel_id=1, source_target_pairs={{0,3},{1,2},{2,1},{3,0},{4,7},{5,6},{6,5},{7,4},{8,11},{9,10},{10,... | collective-permute-start | bytes 98312 | tf_op jit(solution)/shard_map/ppermute | solution.py:582
  40.7 1.5 %collective-permute-start.15 = (bf16[128,128]{1,0:T(8,128)(2,1)S(1)}, bf16[128,128]{1,0:T(8,128)(2,1)S(1)}, u32[]{:S(2)}, u32[]{:S(2)}) collective-permute-start(bf16[128,128]{1,0:T(8,128)(2,1)S(1)} %get-tuple-element.52), channel_id=1, source_target_pairs={{0,5},{1,4},{2,7},{3,6},{4,1},{5,0},{6,3},{7,2},{8,13},{9,12},{10,... | collective-permute-start | bytes 98312 | tf_op jit(solution)/shard_map/ppermute | solution.py:582
  42.1 0.2 collective-permute-start.16
  42.4 1.4 %store.1 = f32[8,4,128,128]{3,2,1,0:T(8,128)} custom-call(bf16[128,128]{1,0:T(8,128)(2,1)S(1)} %get-tuple-element.41.after_ref, f32[4,4,128,128]{3,2,1,0:T(8,128)S(1)} %get-tuple-element.54.refs_0_, f32[4,4,128,128]{3,2,1,0:T(8,128)S(1)} %get-tuple-element.55.refs_1_), custom_call_target="tpu_custom_call" | custom-call | flops 1000000000 | bytes 64 | tf_op jit(solution)/shard_map/store/pallas_call | solution.py:336
  43.8 0.0 collective-permute-done.14.refs_1_
  43.8 0.2 collective-permute-done.15.refs_2_
  44.0 2.4 %collective-permute-done.16.refs_3_ = bf16[128,128]{1,0:T(8,128)(2,1)S(1)} collective-permute-done((bf16[128,128]{1,0:T(8,128)(2,1)S(1)}, bf16[128,128]{1,0:T(8,128)(2,1)S(1)}, u32[]{:S(2)}, u32[]{:S(2)}) %collective-permute-start.16) | collective-permute-done | bytes 32800 | tf_op jit(solution)/shard_map/ppermute | solution.py:582
  46.4 0.6 %finish.1 = bf16[256,128]{1,0:T(8,128)(2,1)} custom-call(f32[128,128]{1,0:T(8,128)S(1)} %get-tuple-element.50.refs_0_, bf16[128,128]{1,0:T(8,128)(2,1)S(1)} %collective-permute-done.14.refs_1_, bf16[128,128]{1,0:T(8,128)(2,1)S(1)} %collective-permute-done.15.refs_2_, bf16[128,128]{1,0:T(8,128)(2,1)S(1)} %collective-permute-done.16.refs_3_), custom_call_target="tpu_custom_call" | custom-call | tf_op jit(solution)/shard_map/finish/pallas_call | solution.py:553
  (3 shorter events, 0.1 us)
Async XLA Ops:
  0.6 5.0 %copy-start.1 = (bf16[512,512]{1,0:T(8,128)(2,1)S(1)}, bf16[512,512]{1,0:T(8,128)(2,1)}, u32[]{:S(2)}) copy-start(bf16[512,512]{1,0:T(8,128)(2,1)} %w_ref.1) | copy-start | bytes 1572868
  0.6 8.9 %copy-start = (bf16[512,512]{1,0:T(8,128)(2,1)S(1)}, bf16[512,512]{1,0:T(8,128)(2,1)}, u32[]{:S(2)}) copy-start(bf16[512,512]{1,0:T(8,128)(2,1)} %near_w_ref.1) | copy-start | bytes 1572868
  2.5 14.5 %collective-permute-start = (bf16[1032,128]{1,0:T(8,128)(2,1)S(1)}, bf16[1032,128]{1,0:T(8,128)(2,1)S(1)}, u32[]{:S(2)}, u32[]{:S(2)}) collective-permute-start(bf16[1032,128]{1,0:T(8,128)(2,1)S(1)} %get-tuple-element.31), channel_id=1, source_target_pairs={{0,4},{4,0},{8,12},{12,8},{16,20},{20,16},{24,28},{28,24},{1,5},{5... | collective-permute-start | bytes 792584 | tf_op jit(solution)/shard_map/ppermute | solution.py:586
  5.9 6.2 %collective-permute-start.1 = (bf16[256,128]{1,0:T(8,128)(2,1)S(1)}, bf16[256,128]{1,0:T(8,128)(2,1)S(1)}, u32[]{:S(2)}, u32[]{:S(2)}) collective-permute-start(bf16[256,128]{1,0:T(8,128)(2,1)S(1)} %get-tuple-element.35), channel_id=1, source_target_pairs={{0,24},{4,28},{8,16},{12,20},{16,8},{20,12},{24,0},{28,4},{1,25},{... | collective-permute-start | bytes 196616 | tf_op jit(solution)/shard_map/ppermute | solution.py:591
  9.6 28.0 %collective-permute-start.11 = (bf16[256,512]{1,0:T(8,128)(2,1)S(1)}, bf16[256,512]{1,0:T(8,128)(2,1)S(1)}, u32[]{:S(2)}, u32[]{:S(2)}) collective-permute-start(bf16[256,512]{1,0:T(8,128)(2,1)S(1)} %get-tuple-element.57), channel_id=1, source_target_pairs={{0,4},{4,0},{8,12},{12,8},{16,20},{20,16},{24,28},{28,24},{1,5},{5... | collective-permute-start | bytes 786440 | tf_op jit(solution)/shard_map/ppermute | solution.py:586
  10.2 27.4 %collective-permute-start.12 = (bf16[256,512]{1,0:T(8,128)(2,1)S(1)}, bf16[256,512]{1,0:T(8,128)(2,1)S(1)}, u32[]{:S(2)}, u32[]{:S(2)}) collective-permute-start(bf16[256,512]{1,0:T(8,128)(2,1)S(1)} %get-tuple-element.56), channel_id=1, source_target_pairs={{0,4},{4,0},{8,12},{12,8},{16,20},{20,16},{24,28},{28,24},{1,5},{5... | collective-permute-start | bytes 786440 | tf_op jit(solution)/shard_map/ppermute | solution.py:586
  11.7 5.4 %collective-permute-start.2 = (bf16[256,128]{1,0:T(8,128)(2,1)S(1)}, bf16[256,128]{1,0:T(8,128)(2,1)S(1)}, u32[]{:S(2)}, u32[]{:S(2)}) collective-permute-start(bf16[256,128]{1,0:T(8,128)(2,1)S(1)} %get-tuple-element.36), channel_id=1, source_target_pairs={{0,16},{4,20},{8,24},{12,28},{16,0},{20,4},{24,8},{28,12},{1,17},{... | collective-permute-start | bytes 196616 | tf_op jit(solution)/shard_map/ppermute | solution.py:591
  12.1 5.0 %collective-permute-start.3 = (bf16[256,128]{1,0:T(8,128)(2,1)S(1)}, bf16[256,128]{1,0:T(8,128)(2,1)S(1)}, u32[]{:S(2)}, u32[]{:S(2)}) collective-permute-start(bf16[256,128]{1,0:T(8,128)(2,1)S(1)} %get-tuple-element.37), channel_id=1, source_target_pairs={{0,8},{4,12},{8,0},{12,4},{16,24},{20,28},{24,16},{28,20},{1,9},{5... | collective-permute-start | bytes 196616 | tf_op jit(solution)/shard_map/ppermute | solution.py:591
  17.1 11.0 %copy-start.2 = (f32[512]{0:T(512)S(1)}, f32[512]{0:T(512)}, u32[]{:S(2)}) copy-start(f32[512]{0:T(512)} %param.17) | copy-start | bytes 6148
  17.1 11.0 %copy-start.3 = (f32[512]{0:T(512)S(1)}, f32[512]{0:T(512)}, u32[]{:S(2)}) copy-start(f32[512]{0:T(512)} %param.18) | copy-start | bytes 6148
  17.2 6.7 %collective-permute-start.4 = (bf16[128,128]{1,0:T(8,128)(2,1)S(1)}, bf16[128,128]{1,0:T(8,128)(2,1)S(1)}, u32[]{:S(2)}, u32[]{:S(2)}) collective-permute-start(bf16[128,128]{1,0:T(8,128)(2,1)S(1)} %get-tuple-element.41.after_ref), channel_id=1, source_target_pairs={{0,4},{4,0},{8,12},{12,8},{16,20},{20,16},{24,28},{28,24},{1,5},{5... | collective-permute-start | bytes 98312 | tf_op jit(solution)/shard_map/ppermute | solution.py:586
  17.7 9.6 %collective-permute-start.5 = (bf16[264,128]{1,0:T(8,128)(2,1)S(1)}, bf16[264,128]{1,0:T(8,128)(2,1)S(1)}, u32[]{:S(2)}, u32[]{:S(2)}) collective-permute-start(bf16[264,128]{1,0:T(8,128)(2,1)S(1)} %get-tuple-element.45), channel_id=1, source_target_pairs={{0,24},{4,28},{8,16},{12,20},{16,8},{20,12},{24,0},{28,4},{1,25},{... | collective-permute-start | bytes 202760 | tf_op jit(solution)/shard_map/ppermute | solution.py:591
  21.2 6.2 %collective-permute-start.6 = (bf16[264,128]{1,0:T(8,128)(2,1)S(1)}, bf16[264,128]{1,0:T(8,128)(2,1)S(1)}, u32[]{:S(2)}, u32[]{:S(2)}) collective-permute-start(bf16[264,128]{1,0:T(8,128)(2,1)S(1)} %get-tuple-element.46), channel_id=1, source_target_pairs={{0,16},{4,20},{8,24},{12,28},{16,0},{20,4},{24,8},{28,12},{1,17},{... | collective-permute-start | bytes 202760 | tf_op jit(solution)/shard_map/ppermute | solution.py:591
  23.9 4.3 %collective-permute-start.7 = (bf16[264,128]{1,0:T(8,128)(2,1)S(1)}, bf16[264,128]{1,0:T(8,128)(2,1)S(1)}, u32[]{:S(2)}, u32[]{:S(2)}) collective-permute-start(bf16[264,128]{1,0:T(8,128)(2,1)S(1)} %get-tuple-element.47), channel_id=1, source_target_pairs={{0,8},{4,12},{8,0},{12,4},{16,24},{20,28},{24,16},{28,20},{1,9},{5... | collective-permute-start | bytes 202760 | tf_op jit(solution)/shard_map/ppermute | solution.py:591
  28.8 5.9 %collective-permute-start.8 = (bf16[32,512]{1,0:T(8,128)(2,1)S(1)}, bf16[32,512]{1,0:T(8,128)(2,1)S(1)}, u32[]{:S(2)}, u32[]{:S(2)}) collective-permute-start(bf16[32,512]{1,0:T(8,128)(2,1)S(1)} %recur.1.own_ref), channel_id=1, source_target_pairs={{0,24},{4,28},{8,16},{12,20},{16,8},{20,12},{24,0},{28,4},{1,25},{... | collective-permute-start | bytes 98312 | tf_op jit(solution)/shard_map/ppermute | solution.py:591
  32.7 4.8 %collective-permute-start.9 = (bf16[32,512]{1,0:T(8,128)(2,1)S(1)}, bf16[32,512]{1,0:T(8,128)(2,1)S(1)}, u32[]{:S(2)}, u32[]{:S(2)}) collective-permute-start(bf16[32,512]{1,0:T(8,128)(2,1)S(1)} %recur.1.own_ref), channel_id=1, source_target_pairs={{0,16},{4,20},{8,24},{12,28},{16,0},{20,4},{24,8},{28,12},{1,17},{... | collective-permute-start | bytes 98312 | tf_op jit(solution)/shard_map/ppermute | solution.py:591
  32.7 4.8 %collective-permute-start.10 = (bf16[32,512]{1,0:T(8,128)(2,1)S(1)}, bf16[32,512]{1,0:T(8,128)(2,1)S(1)}, u32[]{:S(2)}, u32[]{:S(2)}) collective-permute-start(bf16[32,512]{1,0:T(8,128)(2,1)S(1)} %recur.1.own_ref), channel_id=1, source_target_pairs={{0,8},{4,12},{8,0},{12,4},{16,24},{20,28},{24,16},{28,20},{1,9},{5... | collective-permute-start | bytes 98312 | tf_op jit(solution)/shard_map/ppermute | solution.py:591
  37.9 1.4 %collective-permute-start.13 = (bf16[512,128]{1,0:T(8,128)(2,1)S(1)}, bf16[512,128]{1,0:T(8,128)(2,1)S(1)}, u32[]{:S(2)}, u32[]{:S(2)}) collective-permute-start(bf16[512,128]{1,0:T(8,128)(2,1)S(1)} %get-tuple-element.49), channel_id=1, source_target_pairs={{0,1},{1,0},{2,3},{3,2},{4,5},{5,4},{6,7},{7,6},{8,9},{9,8},{10,11... | collective-permute-start | bytes 393224 | tf_op jit(solution)/shard_map/ppermute | solution.py:586
  39.4 4.4 %collective-permute-start.14 = (bf16[128,128]{1,0:T(8,128)(2,1)S(1)}, bf16[128,128]{1,0:T(8,128)(2,1)S(1)}, u32[]{:S(2)}, u32[]{:S(2)}) collective-permute-start(bf16[128,128]{1,0:T(8,128)(2,1)S(1)} %get-tuple-element.51), channel_id=1, source_target_pairs={{0,3},{1,2},{2,1},{3,0},{4,7},{5,6},{6,5},{7,4},{8,11},{9,10},{10,... | collective-permute-start | bytes 98312 | tf_op jit(solution)/shard_map/ppermute | solution.py:582
  40.7 3.3 %collective-permute-start.15 = (bf16[128,128]{1,0:T(8,128)(2,1)S(1)}, bf16[128,128]{1,0:T(8,128)(2,1)S(1)}, u32[]{:S(2)}, u32[]{:S(2)}) collective-permute-start(bf16[128,128]{1,0:T(8,128)(2,1)S(1)} %get-tuple-element.52), channel_id=1, source_target_pairs={{0,5},{1,4},{2,7},{3,6},{4,1},{5,0},{6,3},{7,2},{8,13},{9,12},{10,... | collective-permute-start | bytes 98312 | tf_op jit(solution)/shard_map/ppermute | solution.py:582
  42.1 4.3 %collective-permute-start.16 = (bf16[128,128]{1,0:T(8,128)(2,1)S(1)}, bf16[128,128]{1,0:T(8,128)(2,1)S(1)}, u32[]{:S(2)}, u32[]{:S(2)}) collective-permute-start(bf16[128,128]{1,0:T(8,128)(2,1)S(1)} %get-tuple-element.53), channel_id=1, source_target_pairs={{0,7},{1,6},{2,5},{3,4},{4,3},{5,2},{6,1},{7,0},{8,15},{9,14},{10,... | collective-permute-start | bytes 98312 | tf_op jit(solution)/shard_map/ppermute | solution.py:582

commit v3 on v2

--- a/solution.py
+++ b/solution.py
@@ -620,7 +620,8 @@
         moved.append(along(ahead[k - 1], k, parts))
     ahead = moved
     cut = w_out.shape[0] // 2
-    upper = swap(w_out[:cut], "kv", parts)
+    upper = cross(w_out[:cut], parts, groups, pair=1)
+    aside = swap(w_out, "tp", groups)
     state = (prior_state, prev_forget, prev_values)
     seqs = prior_state.shape[0]
     early = seqs // 2
@@ -634,7 +635,7 @@
         arrived.append(along(sends[k - 1], k, parts))
     base_state = store(pair, (base, late_base))
     other = swap(pair, "kv", parts)
-    lower = swap(w_out[cut:], "kv", parts)
+    lower = cross(w_out[cut:], parts, groups, pair=1)
     normed = recur(
         kept,
         squares,
@@ -650,9 +651,10 @@
     )
     column = []
     for k in order:
-        column.append(along(normed, k, parts))
+        column.append(cross(normed, parts, groups, outer=k))
+    beside = swap(normed, "tp", groups)
     near = stack(column)
-    keep, send = mix(normed, near, w_out, upper, lower, groups)
+    keep, send = mix(beside, near, aside, upper, lower, groups)
     own, sends = join(keep, swap(send, "tp", groups), groups)
     half = groups // PAIR
     pieces = [own] + [None] * (groups - 1)

time: 47.2 us -> 52.7 us (1.12)
  waiting for transfers between devices: 14.8 us -> 19.4 us
  starting transfers between devices: 22.7 us -> 23.6 us
    ppermute x3 -> x8, waiting for transfers between devices: 2.64 us -> 7.98 us  [cross(): return lax.ppermute(x, ('kv', 'tp'), moves)]
    ppermute x3 -> x8, starting transfers between devices: 3.03 us -> 6.76 us  [cross(): return lax.ppermute(x, ('kv', 'tp'), moves)]
    ppermute x9 -> x6, waiting for transfers between devices: 8.16 us -> 5.7 us  [along(): lax.ppermute(x, 'kv', [(s, PAIR * target(s // PAIR, k, count) + s % PAIR)...]
    ppermute x5, waiting for transfers between devices: 4 us -> 5.71 us  [swap(): lax.ppermute(x, axis, [(s, s - s % PAIR + (s + 1) % PAIR) for s in range(...]
    ppermute x5, starting transfers between devices: 5.8 us -> 4.34 us  [swap(): lax.ppermute(x, axis, [(s, s - s % PAIR + (s + 1) % PAIR) for s in range(...]
    ppermute x9 -> x6, starting transfers between devices: 13.9 us -> 12.5 us  [along(): lax.ppermute(x, 'kv', [(s, PAIR * target(s // PAIR, k, count) + s % PAIR)...]
  transfers between devices with their start and end apart: 17 -> 19, of which waited for: 9 -> 10; matrix products, arithmetic and copies ran while one was open for 0% -> 0% of each run, Pallas kernels for 12% -> 11%
where the time goes in v3:
time: 52.7 us; the launch traced here: 52.5 us
  starting transfers between devices  23.6 us (45%)
  waiting for transfers between devices  19.4 us (37%)
  Pallas kernels  8.72 us (17%)
  between operations  0.81 us (2%)
    ppermute x6, starting transfers between devices, along(): lax.ppermute(x, 'kv', [(s, PAIR * target(s // PAIR, k, count) + s % PAIR)...  12.5 us
    ppermute x8, waiting for transfers between devices, cross(): return lax.ppermute(x, ('kv', 'tp'), moves)  7.98 us
    ppermute x8, starting transfers between devices, cross(): return lax.ppermute(x, ('kv', 'tp'), moves)  6.76 us
    ppermute x5, waiting for transfers between devices, swap(): lax.ppermute(x, axis, [(s, s - s % PAIR + (s + 1) % PAIR) for s in range(...  5.71 us
    ppermute x6, waiting for transfers between devices, along(): lax.ppermute(x, 'kv', [(s, PAIR * target(s // PAIR, k, count) + s % PAIR)...  5.7 us
    ppermute x5, starting transfers between devices, swap(): lax.ppermute(x, axis, [(s, s - s % PAIR + (s + 1) % PAIR) for s in range(...  4.34 us
    pallas_call x2, Pallas kernels, fold(): pl.pallas_call(functools.partial(fold_kernel, start), out_shape=[jax.Shap...  3.42 us
    pallas_call x1, Pallas kernels, project(): pl.pallas_call(functools.partial(project_kernel, outer), out_shape=[jax.S...  1.86 us
  transfers between devices with their start and end apart: 19, of which 10 were waited for; matrix products, arithmetic and copies ran while one was open for 0% of the time, Pallas kernels for 11%

profile of v3, /device:TPU:0, one launch (start us, length us, event | category | flops | bytes accessed | tf_op | source)
XLA Modules:
  0.0 52.5 jit_solution(4885309233090456858)
XLA Ops:
  0.6 0.0 copy-start
  0.6 0.0 copy-start.3
  0.7 1.9 %project.1 = (bf16[1032,128]{1,0:T(8,128)(2,1)S(1)}, f32[1024,128]{1,0:T(8,128)S(1)}, f32[2,128]{1,0:T(2,128)S(1)}, bf16[256,512]{1,0:T(8,128)(2,1)S(1)}) custom-call(bf16[256,512]{1,0:T(8,128)(2,1)} %x_hbm.1, bf16[512]{0:T(512)(128)(2,1)} %gain_hbm.1, bf16[512,512]{1,0:T(8,128)(2,1)} %wf_hbm.1, bf16[512,512]{1,0:T(8,128)(2,1)} %wv_hbm.1), custom_call_target="tpu_custom_call" | custom-call | flops 2000000000 | bytes 1048576 | tf_op jit(solution)/shard_map/project/pallas_call | solution.py:118
  2.5 3.1 %collective-permute-start = (bf16[1032,128]{1,0:T(8,128)(2,1)S(1)}, bf16[1032,128]{1,0:T(8,128)(2,1)S(1)}, u32[]{:S(2)}, u32[]{:S(2)}) collective-permute-start(bf16[1032,128]{1,0:T(8,128)(2,1)S(1)} %get-tuple-element.31), channel_id=1, source_target_pairs={{0,4},{4,0},{8,12},{12,8},{16,20},{20,16},{24,28},{28,24},{1,5},{5... | collective-permute-start | bytes 792584 | tf_op jit(solution)/shard_map/ppermute | solution.py:586
  5.6 0.0 copy-done
  5.6 0.3 query.1
  5.9 3.7 %collective-permute-start.1 = (bf16[256,128]{1,0:T(8,128)(2,1)S(1)}, bf16[256,128]{1,0:T(8,128)(2,1)S(1)}, u32[]{:S(2)}, u32[]{:S(2)}) collective-permute-start(bf16[256,128]{1,0:T(8,128)(2,1)S(1)} %get-tuple-element.35), channel_id=1, source_target_pairs={{0,24},{4,28},{8,16},{12,20},{16,8},{20,12},{24,0},{28,4},{1,25},{... | collective-permute-start | bytes 196616 | tf_op jit(solution)/shard_map/ppermute | solution.py:591
  9.6 0.0 collective-permute-start.2
  9.6 0.8 %collective-permute-start.3 = (bf16[256,128]{1,0:T(8,128)(2,1)S(1)}, bf16[256,128]{1,0:T(8,128)(2,1)S(1)}, u32[]{:S(2)}, u32[]{:S(2)}) collective-permute-start(bf16[256,128]{1,0:T(8,128)(2,1)S(1)} %get-tuple-element.37), channel_id=1, source_target_pairs={{0,8},{4,12},{8,0},{12,4},{16,24},{20,28},{24,16},{28,20},{1,9},{5... | collective-permute-start | bytes 196616 | tf_op jit(solution)/shard_map/ppermute | solution.py:591
  10.3 0.0 copy-done.3
  10.3 0.0 collective-permute-start.12
  10.4 2.4 %collective-permute-done.1.refs_4_ = bf16[256,128]{1,0:T(8,128)(2,1)S(1)} collective-permute-done((bf16[256,128]{1,0:T(8,128)(2,1)S(1)}, bf16[256,128]{1,0:T(8,128)(2,1)S(1)}, u32[]{:S(2)}, u32[]{:S(2)}) %collective-permute-start.1) | collective-permute-done | bytes 65568 | tf_op jit(solution)/shard_map/ppermute | solution.py:591
  12.8 0.0 collective-permute-start.13
  12.8 2.2 %collective-permute-done.2.refs_5_ = bf16[256,128]{1,0:T(8,128)(2,1)S(1)} collective-permute-done((bf16[256,128]{1,0:T(8,128)(2,1)S(1)}, bf16[256,128]{1,0:T(8,128)(2,1)S(1)}, u32[]{:S(2)}, u32[]{:S(2)}) %collective-permute-start.2) | collective-permute-done | bytes 65568 | tf_op jit(solution)/shard_map/ppermute | solution.py:591
  15.0 0.0 collective-permute-start.14
  15.0 1.7 %fold.2 = (f32[4,4,128,128]{3,2,1,0:T(8,128)S(1)}, bf16[4,4,128,128]{3,2,1,0:T(8,128)(2,1)S(1)}, bf16[4,4,128,128]{3,2,1,0:T(8,128)(2,1)S(1)}) custom-call(s32[8]{0:T(128)} %accepted_hbm.3, f32[1024,128]{1,0:T(8,128)S(1)} %get-tuple-element.29.after_ref.refs_1_, f32[8,4,128,128]{3,2,1,0:T(8,128)} %state_hbm.3, f32[8,4,512]{2,1,0:T(4,128)} %gate_hbm.3, ...), custom_call_target="tpu_custom_call" | custom-call | flops 1000000000 | bytes 6291456 | tf_op jit(solution)/shard_map/fold/pallas_call | solution.py:289
  16.7 0.0 collective-permute-done.3.refs_6_
  16.7 0.0 collective-permute-done.refs_0_
  16.7 0.1 combine.1
  16.8 0.0 copy-start.1
  16.8 0.0 copy-start.2
  16.9 3.2 %collective-permute-start.5 = (bf16[264,128]{1,0:T(8,128)(2,1)S(1)}, bf16[264,128]{1,0:T(8,128)(2,1)S(1)}, u32[]{:S(2)}, u32[]{:S(2)}) collective-permute-start(bf16[264,128]{1,0:T(8,128)(2,1)S(1)} %get-tuple-element.45), channel_id=1, source_target_pairs={{0,24},{4,28},{8,16},{12,20},{16,8},{20,12},{24,0},{28,4},{1,25},{... | collective-permute-start | bytes 202760 | tf_op jit(solution)/shard_map/ppermute | solution.py:591
  20.1 0.5 collective-permute-start.4
  20.6 4.6 %collective-permute-done.4.refs_3_ = bf16[128,128]{1,0:T(8,128)(2,1)S(1)} collective-permute-done((bf16[128,128]{1,0:T(8,128)(2,1)S(1)}, bf16[128,128]{1,0:T(8,128)(2,1)S(1)}, u32[]{:S(2)}, u32[]{:S(2)}) %collective-permute-start.4) | collective-permute-done | bytes 32800 | tf_op jit(solution)/shard_map/ppermute | solution.py:586
  25.2 3.0 %collective-permute-start.6 = (bf16[264,128]{1,0:T(8,128)(2,1)S(1)}, bf16[264,128]{1,0:T(8,128)(2,1)S(1)}, u32[]{:S(2)}, u32[]{:S(2)}) collective-permute-start(bf16[264,128]{1,0:T(8,128)(2,1)S(1)} %get-tuple-element.46), channel_id=1, source_target_pairs={{0,16},{4,20},{8,24},{12,28},{16,0},{20,4},{24,8},{28,12},{1,17},{... | collective-permute-start | bytes 202760 | tf_op jit(solution)/shard_map/ppermute | solution.py:591
  28.2 0.0 collective-permute-done.5.refs_8_
  28.2 1.8 %collective-permute-start.7 = (bf16[264,128]{1,0:T(8,128)(2,1)S(1)}, bf16[264,128]{1,0:T(8,128)(2,1)S(1)}, u32[]{:S(2)}, u32[]{:S(2)}) collective-permute-start(bf16[264,128]{1,0:T(8,128)(2,1)S(1)} %get-tuple-element.47), channel_id=1, source_target_pairs={{0,8},{4,12},{8,0},{12,4},{16,24},{20,28},{24,16},{28,20},{1,9},{5... | collective-permute-start | bytes 202760 | tf_op jit(solution)/shard_map/ppermute | solution.py:591
  30.0 1.7 %fold.3 = (f32[4,4,128,128]{3,2,1,0:T(8,128)S(1)}, bf16[4,4,128,128]{3,2,1,0:T(8,128)(2,1)S(1)}, bf16[4,4,128,128]{3,2,1,0:T(8,128)(2,1)S(1)}) custom-call(s32[8]{0:T(128)} %accepted_hbm.3, bf16[128,128]{1,0:T(8,128)(2,1)S(1)} %get-tuple-element.41.after_ref, f32[8,4,128,128]{3,2,1,0:T(8,128)} %state_hbm.3, f32[8,4,512]{2,1,0:T(4,128)} %gate_hbm.3, ...), custom_call_target="tpu_custom_call" | custom-call | flops 1000000000 | bytes 6291456 | tf_op jit(solution)/shard_map/fold/pallas_call | solution.py:289
  31.7 0.0 collective-permute-done.6.refs_9_
  31.7 1.1 %collective-permute-done.7.refs_10_ = bf16[264,128]{1,0:T(8,128)(2,1)S(1)} collective-permute-done((bf16[264,128]{1,0:T(8,128)(2,1)S(1)}, bf16[264,128]{1,0:T(8,128)(2,1)S(1)}, u32[]{:S(2)}, u32[]{:S(2)}) %collective-permute-start.7) | collective-permute-done | bytes 67616 | tf_op jit(solution)/shard_map/ppermute | solution.py:591
  32.8 0.0 copy-done.1
  32.8 0.0 copy-done.2
  32.9 0.7 %recur.1 = bf16[32,512]{1,0:T(8,128)(2,1)S(1)} custom-call(f32[256,128]{1,0:T(8,128)S(1)} %get-tuple-element.38.refs_0_, f32[2,128]{1,0:T(2,128)S(1)} %get-tuple-element.39.refs_1_, f32[128,128]{1,0:T(8,128)S(1)} %get-tuple-element.40.refs_2_, bf16[128,128]{1,0:T(8,128)(2,1)S(1)} %collective-permute-done.4.refs_3_, ...), custom_call_target="tpu_custom_call" | custom-call | tf_op jit(solution)/shard_map/recur/pallas_call | solution.py:432
  33.5 3.2 %collective-permute-start.9 = (bf16[32,512]{1,0:T(8,128)(2,1)S(1)}, bf16[32,512]{1,0:T(8,128)(2,1)S(1)}, u32[]{:S(2)}, u32[]{:S(2)}) collective-permute-start(bf16[32,512]{1,0:T(8,128)(2,1)S(1)} %recur.1), channel_id=1, source_target_pairs={{0,25},{1,24},{2,27},{3,26},{4,29},{5,28},{6,31},{7,30},{8,17},{9,... | collective-permute-start | bytes 98312 | tf_op jit(solution)/shard_map/ppermute | solution.py:582
  36.7 0.0 collective-permute-start.10
  36.7 2.2 %collective-permute-done.9.refs_0_ = bf16[32,512]{1,0:T(8,128)(2,1)S(1)} collective-permute-done((bf16[32,512]{1,0:T(8,128)(2,1)S(1)}, bf16[32,512]{1,0:T(8,128)(2,1)S(1)}, u32[]{:S(2)}, u32[]{:S(2)}) %collective-permute-start.9) | collective-permute-done | bytes 32800 | tf_op jit(solution)/shard_map/ppermute | solution.py:582
  38.9 0.0 collective-permute-start.11
  38.9 2.1 %collective-permute-done.10.refs_1_ = bf16[32,512]{1,0:T(8,128)(2,1)S(1)} collective-permute-done((bf16[32,512]{1,0:T(8,128)(2,1)S(1)}, bf16[32,512]{1,0:T(8,128)(2,1)S(1)}, u32[]{:S(2)}, u32[]{:S(2)}) %collective-permute-start.10) | collective-permute-done | bytes 32800 | tf_op jit(solution)/shard_map/ppermute | solution.py:582
  40.9 0.4 collective-permute-start.8
  41.4 0.9 %collective-permute-done.11.refs_2_ = bf16[32,512]{1,0:T(8,128)(2,1)S(1)} collective-permute-done((bf16[32,512]{1,0:T(8,128)(2,1)S(1)}, bf16[32,512]{1,0:T(8,128)(2,1)S(1)}, u32[]{:S(2)}, u32[]{:S(2)}) %collective-permute-start.11) | collective-permute-done | bytes 32800 | tf_op jit(solution)/shard_map/ppermute | solution.py:582
  42.2 0.0 collective-permute-done.13.upper_ref
  42.3 0.0 collective-permute-done.14.lower_ref
  42.3 0.0 collective-permute-done.8.own_ref
  42.3 0.0 collective-permute-done.12.near_w_ref
  42.3 0.3 mix.1
  42.6 0.3 collective-permute-start.15
  43.0 1.1 %collective-permute-done.15.other_ref = bf16[512,128]{1,0:T(8,128)(2,1)S(1)} collective-permute-done((bf16[512,128]{1,0:T(8,128)(2,1)S(1)}, bf16[512,128]{1,0:T(8,128)(2,1)S(1)}, u32[]{:S(2)}, u32[]{:S(2)}) %collective-permute-start.15) | collective-permute-done | bytes 131104 | tf_op jit(solution)/shard_map/ppermute | solution.py:586
  44.1 2.0 %collective-permute-start.16 = (bf16[128,128]{1,0:T(8,128)(2,1)S(1)}, bf16[128,128]{1,0:T(8,128)(2,1)S(1)}, u32[]{:S(2)}, u32[]{:S(2)}) collective-permute-start(bf16[128,128]{1,0:T(8,128)(2,1)S(1)} %get-tuple-element.51), channel_id=1, source_target_pairs={{0,3},{1,2},{2,1},{3,0},{4,7},{5,6},{6,5},{7,4},{8,11},{9,10},{10,... | collective-permute-start | bytes 98312 | tf_op jit(solution)/shard_map/ppermute | solution.py:582
  46.1 1.6 %collective-permute-start.17 = (bf16[128,128]{1,0:T(8,128)(2,1)S(1)}, bf16[128,128]{1,0:T(8,128)(2,1)S(1)}, u32[]{:S(2)}, u32[]{:S(2)}) collective-permute-start(bf16[128,128]{1,0:T(8,128)(2,1)S(1)} %get-tuple-element.52), channel_id=1, source_target_pairs={{0,5},{1,4},{2,7},{3,6},{4,1},{5,0},{6,3},{7,2},{8,13},{9,12},{10,... | collective-permute-start | bytes 98312 | tf_op jit(solution)/shard_map/ppermute | solution.py:582
  47.6 0.0 collective-permute-start.18
  47.6 1.4 %store.1 = f32[8,4,128,128]{3,2,1,0:T(8,128)} custom-call(bf16[128,128]{1,0:T(8,128)(2,1)S(1)} %get-tuple-element.41.after_ref, f32[4,4,128,128]{3,2,1,0:T(8,128)S(1)} %get-tuple-element.54.refs_0_, f32[4,4,128,128]{3,2,1,0:T(8,128)S(1)} %get-tuple-element.55.refs_1_), custom_call_target="tpu_custom_call" | custom-call | flops 1000000000 | bytes 64 | tf_op jit(solution)/shard_map/store/pallas_call | solution.py:336
  49.0 0.0 collective-permute-done.16.refs_1_
  49.0 0.4 collective-permute-done.17.refs_2_
  49.4 2.5 %collective-permute-done.18.refs_3_ = bf16[128,128]{1,0:T(8,128)(2,1)S(1)} collective-permute-done((bf16[128,128]{1,0:T(8,128)(2,1)S(1)}, bf16[128,128]{1,0:T(8,128)(2,1)S(1)}, u32[]{:S(2)}, u32[]{:S(2)}) %collective-permute-start.18) | collective-permute-done | bytes 32800 | tf_op jit(solution)/shard_map/ppermute | solution.py:582
  51.9 0.6 %finish.1 = bf16[256,128]{1,0:T(8,128)(2,1)} custom-call(f32[128,128]{1,0:T(8,128)S(1)} %get-tuple-element.50.refs_0_, bf16[128,128]{1,0:T(8,128)(2,1)S(1)} %collective-permute-done.16.refs_1_, bf16[128,128]{1,0:T(8,128)(2,1)S(1)} %collective-permute-done.17.refs_2_, bf16[128,128]{1,0:T(8,128)(2,1)S(1)} %collective-permute-done.18.refs_3_), custom_call_target="tpu_custom_call" | custom-call | tf_op jit(solution)/shard_map/finish/pallas_call | solution.py:553
  (3 shorter events, 0.1 us)
Async XLA Ops:
  0.6 5.0 %copy-start = (bf16[512,512]{1,0:T(8,128)(2,1)S(1)}, bf16[512,512]{1,0:T(8,128)(2,1)}, u32[]{:S(2)}) copy-start(bf16[512,512]{1,0:T(8,128)(2,1)} %w_ref.1) | copy-start | bytes 1572868
  0.6 9.7 %copy-start.3 = (bf16[512,512]{1,0:T(8,128)(2,1)S(1)}, bf16[512,512]{1,0:T(8,128)(2,1)}, u32[]{:S(2)}) copy-start(bf16[512,512]{1,0:T(8,128)(2,1)} %param.19) | copy-start | bytes 1572868
  2.5 14.2 %collective-permute-start = (bf16[1032,128]{1,0:T(8,128)(2,1)S(1)}, bf16[1032,128]{1,0:T(8,128)(2,1)S(1)}, u32[]{:S(2)}, u32[]{:S(2)}) collective-permute-start(bf16[1032,128]{1,0:T(8,128)(2,1)S(1)} %get-tuple-element.31), channel_id=1, source_target_pairs={{0,4},{4,0},{8,12},{12,8},{16,20},{20,16},{24,28},{28,24},{1,5},{5... | collective-permute-start | bytes 792584 | tf_op jit(solution)/shard_map/ppermute | solution.py:586
  5.9 6.9 %collective-permute-start.1 = (bf16[256,128]{1,0:T(8,128)(2,1)S(1)}, bf16[256,128]{1,0:T(8,128)(2,1)S(1)}, u32[]{:S(2)}, u32[]{:S(2)}) collective-permute-start(bf16[256,128]{1,0:T(8,128)(2,1)S(1)} %get-tuple-element.35), channel_id=1, source_target_pairs={{0,24},{4,28},{8,16},{12,20},{16,8},{20,12},{24,0},{28,4},{1,25},{... | collective-permute-start | bytes 196616 | tf_op jit(solution)/shard_map/ppermute | solution.py:591
  9.6 5.4 %collective-permute-start.2 = (bf16[256,128]{1,0:T(8,128)(2,1)S(1)}, bf16[256,128]{1,0:T(8,128)(2,1)S(1)}, u32[]{:S(2)}, u32[]{:S(2)}) collective-permute-start(bf16[256,128]{1,0:T(8,128)(2,1)S(1)} %get-tuple-element.36), channel_id=1, source_target_pairs={{0,16},{4,20},{8,24},{12,28},{16,0},{20,4},{24,8},{28,12},{1,17},{... | collective-permute-start | bytes 196616 | tf_op jit(solution)/shard_map/ppermute | solution.py:591
  9.6 7.2 %collective-permute-start.3 = (bf16[256,128]{1,0:T(8,128)(2,1)S(1)}, bf16[256,128]{1,0:T(8,128)(2,1)S(1)}, u32[]{:S(2)}, u32[]{:S(2)}) collective-permute-start(bf16[256,128]{1,0:T(8,128)(2,1)S(1)} %get-tuple-element.37), channel_id=1, source_target_pairs={{0,8},{4,12},{8,0},{12,4},{16,24},{20,28},{24,16},{28,20},{1,9},{5... | collective-permute-start | bytes 196616 | tf_op jit(solution)/shard_map/ppermute | solution.py:591
  10.3 31.9 %collective-permute-start.12 = (bf16[512,512]{1,0:T(8,128)(2,1)S(1)}, bf16[512,512]{1,0:T(8,128)(2,1)S(1)}, u32[]{:S(2)}, u32[]{:S(2)}) collective-permute-start(bf16[512,512]{1,0:T(8,128)(2,1)S(1)} %copy-done.3), channel_id=1, source_target_pairs={{0,1},{1,0},{2,3},{3,2},{4,5},{5,4},{6,7},{7,6},{8,9},{9,8},{10,11... | collective-permute-start | bytes 1572872 | tf_op jit(solution)/shard_map/ppermute | solution.py:586
  12.8 29.4 %collective-permute-start.13 = (bf16[256,512]{1,0:T(8,128)(2,1)S(1)}, bf16[256,512]{1,0:T(8,128)(2,1)S(1)}, u32[]{:S(2)}, u32[]{:S(2)}) collective-permute-start(bf16[256,512]{1,0:T(8,128)(2,1)S(1)} %get-tuple-element.57), channel_id=1, source_target_pairs={{0,5},{1,4},{2,7},{3,6},{4,1},{5,0},{6,3},{7,2},{8,13},{9,12},{10,... | collective-permute-start | bytes 786440 | tf_op jit(solution)/shard_map/ppermute | solution.py:582
  15.0 27.3 %collective-permute-start.14 = (bf16[256,512]{1,0:T(8,128)(2,1)S(1)}, bf16[256,512]{1,0:T(8,128)(2,1)S(1)}, u32[]{:S(2)}, u32[]{:S(2)}) collective-permute-start(bf16[256,512]{1,0:T(8,128)(2,1)S(1)} %get-tuple-element.56), channel_id=1, source_target_pairs={{0,5},{1,4},{2,7},{3,6},{4,1},{5,0},{6,3},{7,2},{8,13},{9,12},{10,... | collective-permute-start | bytes 786440 | tf_op jit(solution)/shard_map/ppermute | solution.py:582
  16.8 16.0 %copy-start.1 = (f32[512]{0:T(512)S(1)}, f32[512]{0:T(512)}, u32[]{:S(2)}) copy-start(f32[512]{0:T(512)} %param.17) | copy-start | bytes 6148
  16.8 16.0 %copy-start.2 = (f32[512]{0:T(512)S(1)}, f32[512]{0:T(512)}, u32[]{:S(2)}) copy-start(f32[512]{0:T(512)} %param.18) | copy-start | bytes 6148
  16.9 11.4 %collective-permute-start.5 = (bf16[264,128]{1,0:T(8,128)(2,1)S(1)}, bf16[264,128]{1,0:T(8,128)(2,1)S(1)}, u32[]{:S(2)}, u32[]{:S(2)}) collective-permute-start(bf16[264,128]{1,0:T(8,128)(2,1)S(1)} %get-tuple-element.45), channel_id=1, source_target_pairs={{0,24},{4,28},{8,16},{12,20},{16,8},{20,12},{24,0},{28,4},{1,25},{... | collective-permute-start | bytes 202760 | tf_op jit(solution)/shard_map/ppermute | solution.py:591
  20.1 5.1 %collective-permute-start.4 = (bf16[128,128]{1,0:T(8,128)(2,1)S(1)}, bf16[128,128]{1,0:T(8,128)(2,1)S(1)}, u32[]{:S(2)}, u32[]{:S(2)}) collective-permute-start(bf16[128,128]{1,0:T(8,128)(2,1)S(1)} %get-tuple-element.41.after_ref), channel_id=1, source_target_pairs={{0,4},{4,0},{8,12},{12,8},{16,20},{20,16},{24,28},{28,24},{1,5},{5... | collective-permute-start | bytes 98312 | tf_op jit(solution)/shard_map/ppermute | solution.py:586
  25.2 6.5 %collective-permute-start.6 = (bf16[264,128]{1,0:T(8,128)(2,1)S(1)}, bf16[264,128]{1,0:T(8,128)(2,1)S(1)}, u32[]{:S(2)}, u32[]{:S(2)}) collective-permute-start(bf16[264,128]{1,0:T(8,128)(2,1)S(1)} %get-tuple-element.46), channel_id=1, source_target_pairs={{0,16},{4,20},{8,24},{12,28},{16,0},{20,4},{24,8},{28,12},{1,17},{... | collective-permute-start | bytes 202760 | tf_op jit(solution)/shard_map/ppermute | solution.py:591
  28.2 4.6 %collective-permute-start.7 = (bf16[264,128]{1,0:T(8,128)(2,1)S(1)}, bf16[264,128]{1,0:T(8,128)(2,1)S(1)}, u32[]{:S(2)}, u32[]{:S(2)}) collective-permute-start(bf16[264,128]{1,0:T(8,128)(2,1)S(1)} %get-tuple-element.47), channel_id=1, source_target_pairs={{0,8},{4,12},{8,0},{12,4},{16,24},{20,28},{24,16},{28,20},{1,9},{5... | collective-permute-start | bytes 202760 | tf_op jit(solution)/shard_map/ppermute | solution.py:591
  33.5 5.4 %collective-permute-start.9 = (bf16[32,512]{1,0:T(8,128)(2,1)S(1)}, bf16[32,512]{1,0:T(8,128)(2,1)S(1)}, u32[]{:S(2)}, u32[]{:S(2)}) collective-permute-start(bf16[32,512]{1,0:T(8,128)(2,1)S(1)} %recur.1), channel_id=1, source_target_pairs={{0,25},{1,24},{2,27},{3,26},{4,29},{5,28},{6,31},{7,30},{8,17},{9,... | collective-permute-start | bytes 98312 | tf_op jit(solution)/shard_map/ppermute | solution.py:582
  36.7 4.2 %collective-permute-start.10 = (bf16[32,512]{1,0:T(8,128)(2,1)S(1)}, bf16[32,512]{1,0:T(8,128)(2,1)S(1)}, u32[]{:S(2)}, u32[]{:S(2)}) collective-permute-start(bf16[32,512]{1,0:T(8,128)(2,1)S(1)} %recur.1), channel_id=1, source_target_pairs={{0,17},{1,16},{2,19},{3,18},{4,21},{5,20},{6,23},{7,22},{8,25},{9,... | collective-permute-start | bytes 98312 | tf_op jit(solution)/shard_map/ppermute | solution.py:582
  38.9 3.3 %collective-permute-start.11 = (bf16[32,512]{1,0:T(8,128)(2,1)S(1)}, bf16[32,512]{1,0:T(8,128)(2,1)S(1)}, u32[]{:S(2)}, u32[]{:S(2)}) collective-permute-start(bf16[32,512]{1,0:T(8,128)(2,1)S(1)} %recur.1), channel_id=1, source_target_pairs={{0,9},{1,8},{2,11},{3,10},{4,13},{5,12},{6,15},{7,14},{8,1},{9,0},... | collective-permute-start | bytes 98312 | tf_op jit(solution)/shard_map/ppermute | solution.py:582
  40.9 1.3 %collective-permute-start.8 = (bf16[32,512]{1,0:T(8,128)(2,1)S(1)}, bf16[32,512]{1,0:T(8,128)(2,1)S(1)}, u32[]{:S(2)}, u32[]{:S(2)}) collective-permute-start(bf16[32,512]{1,0:T(8,128)(2,1)S(1)} %recur.1), channel_id=1, source_target_pairs={{0,1},{1,0},{2,3},{3,2},{4,5},{5,4},{6,7},{7,6},{8,9},{9,8},{10,11... | collective-permute-start | bytes 98312 | tf_op jit(solution)/shard_map/ppermute | solution.py:586
  42.6 1.4 %collective-permute-start.15 = (bf16[512,128]{1,0:T(8,128)(2,1)S(1)}, bf16[512,128]{1,0:T(8,128)(2,1)S(1)}, u32[]{:S(2)}, u32[]{:S(2)}) collective-permute-start(bf16[512,128]{1,0:T(8,128)(2,1)S(1)} %get-tuple-element.49), channel_id=1, source_target_pairs={{0,1},{1,0},{2,3},{3,2},{4,5},{5,4},{6,7},{7,6},{8,9},{9,8},{10,11... | collective-permute-start | bytes 393224 | tf_op jit(solution)/shard_map/ppermute | solution.py:586
  44.1 4.9 %collective-permute-start.16 = (bf16[128,128]{1,0:T(8,128)(2,1)S(1)}, bf16[128,128]{1,0:T(8,128)(2,1)S(1)}, u32[]{:S(2)}, u32[]{:S(2)}) collective-permute-start(bf16[128,128]{1,0:T(8,128)(2,1)S(1)} %get-tuple-element.51), channel_id=1, source_target_pairs={{0,3},{1,2},{2,1},{3,0},{4,7},{5,6},{6,5},{7,4},{8,11},{9,10},{10,... | collective-permute-start | bytes 98312 | tf_op jit(solution)/shard_map/ppermute | solution.py:582
  46.1 3.3 %collective-permute-start.17 = (bf16[128,128]{1,0:T(8,128)(2,1)S(1)}, bf16[128,128]{1,0:T(8,128)(2,1)S(1)}, u32[]{:S(2)}, u32[]{:S(2)}) collective-permute-start(bf16[128,128]{1,0:T(8,128)(2,1)S(1)} %get-tuple-element.52), channel_id=1, source_target_pairs={{0,5},{1,4},{2,7},{3,6},{4,1},{5,0},{6,3},{7,2},{8,13},{9,12},{10,... | collective-permute-start | bytes 98312 | tf_op jit(solution)/shard_map/ppermute | solution.py:582
  47.6 4.3 %collective-permute-start.18 = (bf16[128,128]{1,0:T(8,128)(2,1)S(1)}, bf16[128,128]{1,0:T(8,128)(2,1)S(1)}, u32[]{:S(2)}, u32[]{:S(2)}) collective-permute-start(bf16[128,128]{1,0:T(8,128)(2,1)S(1)} %get-tuple-element.53), channel_id=1, source_target_pairs={{0,7},{1,6},{2,5},{3,4},{4,3},{5,2},{6,1},{7,0},{8,15},{9,14},{10,... | collective-permute-start | bytes 98312 | tf_op jit(solution)/shard_map/ppermute | solution.py:582
